TPU v7x, 256 devices: a whole 4x4x8 slice. The times are simulated.
256 devices in a mesh: sp: 64 (over z, y, core), tp: 4 (over x).
Axes of the slice: x: 4, y: 4, z: 8, core: 2. Of those that a mesh axis runs over, the one named last changes fastest.
Arguments:
- memory_queries: bfloat16 [16384, 768], P('sp', 'tp'), may hold values from -6 to 6
- memory_keys: bfloat16 [16384, 768], P('sp', 'tp'), may hold values from -6 to 6
- memory_values: bfloat16 [16384, 768], P('sp', 'tp'), may hold values from -6 to 6
- output_gate_preactivation: bfloat16 [16384, 768], P('sp', 'tp'), may hold values from -6 to 6
- log_input_gate: float32 [8, 16384], P('tp', 'sp'), may hold values from -4 to 300
- forget_preactivation: float32 [8, 16384], P('tp', 'sp'), may hold values from -5 to 5
- head_forget_bias: float32 [8], P('tp'), may hold values from 3 to 16
- forget_extra_boost: float32 [8, 16384], P('tp', 'sp'), may hold values from -2 to 0
- head_norm_gain: float32 [768], P('tp'), may hold values from 0.1 to 1.9
- memory_output_weight: bfloat16 [768, 2048], replicated, may hold values from -0.21875 to 0.21875
- residual: bfloat16 [16384, 2048], P('sp'), may hold values from -6 to 6
- expert_norm_gain: float32 [2048], replicated, may hold values from 0.1 to 1.9
- routes: int32 [16384, 4], P('sp'), may hold values from 0 to 255, all different within a row; in each aligned block of 256 rows (0 to 255, 256 to 511, ...) at most 8 rows name the same one
- router_weight_matrix: float32 [16384, 4], P('sp'), may hold values from 0.1 to 1
- routed_gate_weight: bfloat16 [256, 2048, 512], P('sp', None, 'tp'), may hold values from -0.125 to 0.125
- routed_up_weight: bfloat16 [256, 2048, 512], P('sp', None, 'tp'), may hold values from -0.125 to 0.125
- routed_down_weight: bfloat16 [256, 512, 2048], P('sp', 'tp'), may hold values from -0.25 to 0.25
- shared_gate_weight: bfloat16 [2048, 512], P(None, 'tp'), may hold values from -0.125 to 0.125
- shared_up_weight: bfloat16 [2048, 512], P(None, 'tp'), may hold values from -0.125 to 0.125
- shared_down_weight: bfloat16 [512, 2048], P('tp'), may hold values from -0.25 to 0.25
Outputs:
- updated: bfloat16 [16384, 2048], P('sp', 'tp')
Inputs may be any that keep to these rules, and one draw needn't show every extreme that they name: `routes`: each row names 4 different experts. In each aligned block of 256 rows (the rows of one index of sp) no expert is named by more than 8 rows, a bound that some block reaches.
All inputs are finite; a program needn't handle non-finite values.
Results may differ from a plain program's by a relative error of at most 0.0085.
Values may be sent and summed in bfloat16 or wider, within the bound.
A program may use at most 128 MiB of HBM per device.

v0:
```python
import jax
import jax.numpy as jnp
from jax import lax
from jax.sharding import Mesh
from jax.sharding import PartitionSpec as P

SP = ("sp_0", "sp_1", "sp_2")


NEG_LARGE = -1e30
EPSILON = 1e-06


def nothing_yet(shard, identity):
    return jax.tree.map(
        lambda a, e: jnp.broadcast_to(jnp.asarray(e, a.dtype), a.shape), shard, identity
    )


def gathered_once(shard, axis):
    leaves = jax.tree.leaves(shard)
    turns = sorted(range(len(leaves)), key=lambda k: -leaves[k].size)
    width = (1, *leaves[turns[0]].shape)[-1]
    lines = [
        jnp.pad(leaves[k].reshape(-1), (0, -leaves[k].size % width)).reshape(-1, width)
        for k in turns
    ]
    both, at, found = (lax.all_gather(jnp.concatenate(lines), axis), 0, {})
    for k, line in zip(turns, lines):
        slab = both[:, at : at + len(line)].reshape(len(both), -1)
        found[k] = slab[:, : leaves[k].size].reshape(-1, *leaves[k].shape)
        at += len(line)
    numbers = iter(range(len(leaves)))
    return jax.tree.map(lambda _: found[next(numbers)], shard)


def entering(shard, axes, combine, identity):
    before = start = nothing_yet(shard, identity)
    subtotal = shard
    for axis in reversed(axes):
        count, here = (lax.axis_size(axis), lax.axis_index(axis))
        pieces = gathered_once(subtotal, axis)
        inside, subtotal = (start, start)
        for k in range(count):
            passed = k < here
            subtotal = combine(subtotal, jax.tree.map(lambda part: part[k], pieces))
            inside = jax.tree.map(lambda new, old: jnp.where(passed, new, old), subtotal, inside)
        before = combine(inside, before)
    return before


def in_one_piece(arrays, axis, split_dim, concat_dim, along):
    ends, at = ([], 0)
    for a in arrays[:-1]:
        at += a.shape[along]
        ends.append(at)
    both = jnp.concatenate(arrays, axis=along)
    return tuple(
        jnp.split(
            lax.all_to_all(both, axis, split_axis=split_dim, concat_axis=concat_dim, tiled=True),
            ends,
            axis=along,
        )
    )


def cut_along(shard, dim, count):
    shape = shard.shape
    blocks = shard.reshape(*shape[:dim], count, shape[dim] // count, *shape[dim + 1 :])
    return jnp.moveaxis(blocks, dim, 0)


def summed_on_arrival(shard, axis, dim):
    count = lax.axis_size(axis)
    blocks = lax.all_to_all(cut_along(shard, dim, count), axis, 0, 0, tiled=True)
    return jnp.sum(blocks.astype(jnp.float32), axis=0)


def join_states(earlier, later):
    memory_a, top_a, total_a = earlier
    memory_b, top_b, total_b = later
    joined = jnp.maximum(total_b + top_a, top_b)
    carry_weight = jnp.exp(total_b + top_a - joined)
    own_weight = jnp.exp(top_b - joined)
    memory = carry_weight[:, None, None] * memory_a + own_weight[:, None, None] * memory_b
    return (memory, joined, total_a + total_b)


def body(
    memory_queries,
    memory_keys,
    memory_values,
    output_gate_preactivation,
    log_input_gate,
    forget_preactivation,
    head_forget_bias,
    forget_extra_boost,
    head_norm_gain,
    memory_output_weight,
    residual,
    expert_norm_gain,
    routes,
    router_weight_matrix,
    routed_gate_weight,
    routed_up_weight,
    routed_down_weight,
    shared_gate_weight,
    shared_up_weight,
    shared_down_weight,
):
    tokens_here = memory_queries.shape[0]
    heads_here = log_input_gate.shape[0]
    head_size = memory_queries.shape[1] // heads_here
    scale = head_size ** (-0.5)
    queries = memory_queries.reshape(tokens_here, heads_here, head_size)
    keyset = memory_keys.reshape(tokens_here, heads_here, head_size)
    valueset = memory_values.reshape(tokens_here, heads_here, head_size)
    forget_log_gate = (
        jax.nn.log_sigmoid(forget_preactivation + head_forget_bias[:, None]) + forget_extra_boost
    )
    cumul = jnp.cumsum(forget_log_gate, axis=1)
    causal = jnp.tril(jnp.ones((tokens_here, tokens_here), bool))
    d_log = jnp.where(
        causal[None], cumul[:, :, None] - cumul[:, None, :] + log_input_gate[:, None, :], NEG_LARGE
    )
    ending = cumul[:, -1]
    w_log = ending[:, None] - cumul + log_input_gate
    local_top = jnp.max(w_log, axis=1)
    w_end = jnp.exp(w_log - local_top[:, None])
    keys_float = keyset.astype(jnp.float32)
    values_float = valueset.astype(jnp.float32)
    local_memory = jnp.einsum(
        "hs,shd,she->hde", w_end, keys_float, values_float, precision=lax.Precision.HIGHEST
    )
    identity = (
        jnp.zeros_like(local_memory),
        jnp.full_like(local_top, NEG_LARGE),
        jnp.zeros_like(ending),
    )
    memory, stabil, _ = entering((local_memory, local_top, ending), SP, join_states, identity)
    g_log = cumul + stabil[:, None]
    top = jnp.maximum(g_log, jnp.max(d_log, axis=2))
    scores = jnp.einsum("thd,shd->hts", queries, keyset, preferred_element_type=jnp.float32) * scale
    weights = scores * jnp.exp(d_log - top[:, :, None])
    inter = jnp.exp(g_log - top)
    q_scaled = queries.astype(jnp.float32) * scale
    numer = jnp.einsum(
        "hts,shd->thd", weights.astype(jnp.bfloat16), valueset, preferred_element_type=jnp.float32
    )
    hidden = numer + inter.T[:, :, None] * jnp.einsum(
        "thd,hde->the", q_scaled, memory, precision=lax.Precision.HIGHEST
    )
    hidden = hidden * lax.rsqrt(jnp.mean(hidden * hidden, axis=2, keepdims=True) + EPSILON)
    token_mixing = (
        hidden.reshape(tokens_here, heads_here * head_size)
        * head_norm_gain
        * jax.nn.sigmoid(output_gate_preactivation.astype(jnp.float32))
    ).astype(jnp.bfloat16)
    model_width = residual.shape[1]
    mixed = jnp.dot(
        lax.all_gather(token_mixing, "tp", axis=1, tiled=True),
        memory_output_weight,
        preferred_element_type=jnp.float32,
    )
    stream = residual.astype(jnp.float32) + mixed
    normed = (
        stream
        * lax.rsqrt(jnp.mean(stream * stream, axis=1, keepdims=True) + EPSILON)
        * expert_norm_gain
    ).astype(jnp.bfloat16)
    sp_count = lax.axis_size(SP)
    tp_count = lax.axis_size("tp")
    tp_index = lax.axis_index("tp")
    local_experts = routed_gate_weight.shape[0]
    experts_total = local_experts * sp_count
    top_count = routes.shape[1]
    capacity = 2 * tokens_here * top_count // experts_total
    width_share = model_width // tp_count
    flat_routes = routes.reshape(-1)
    onehot = (flat_routes[:, None] == jnp.arange(experts_total, dtype=jnp.int32)[None, :]).astype(
        jnp.int32
    )
    earlier_count = jnp.cumsum(onehot, axis=0) - onehot
    slot_index = jnp.sum(earlier_count * onehot, axis=1)
    position = flat_routes * capacity + slot_index
    owner = jnp.arange(flat_routes.shape[0], dtype=jnp.int32) // top_count
    slot_token = (
        jnp.full((experts_total * capacity,), tokens_here, jnp.int32).at[position].set(owner)
    )
    padded = jnp.concatenate([normed, jnp.zeros((1, model_width), jnp.bfloat16)], axis=0)
    shared_hidden = (
        jax.nn.silu(jnp.dot(normed, shared_gate_weight, preferred_element_type=jnp.float32))
        * jnp.dot(normed, shared_up_weight, preferred_element_type=jnp.float32)
    ).astype(jnp.bfloat16)
    shared_partial = jnp.dot(shared_hidden, shared_down_weight, preferred_element_type=jnp.float32)
    stream_share = lax.dynamic_slice_in_dim(stream, tp_index * width_share, width_share, 1)
    group_count = local_experts // tp_count
    whole_gate, whole_up = in_one_piece((routed_gate_weight, routed_up_weight), "tp", 0, 2, 1)
    whole_down = lax.all_to_all(routed_down_weight, "tp", split_axis=0, concat_axis=1, tiled=True)
    slot_table = slot_token.reshape(sp_count, local_experts, capacity)
    chosen = lax.dynamic_slice_in_dim(slot_table, tp_index * group_count, group_count, 1)
    outgoing = jnp.take(padded, chosen.reshape(-1), axis=0).reshape(
        sp_count, group_count, capacity, model_width
    )
    arrived = lax.all_to_all(outgoing, SP, split_axis=0, concat_axis=0, tiled=True)
    gate_vals = jnp.einsum(
        "secd,edf->secf", arrived, whole_gate, preferred_element_type=jnp.float32
    )
    up_vals = jnp.einsum("secd,edf->secf", arrived, whole_up, preferred_element_type=jnp.float32)
    expert_hidden = (jax.nn.silu(gate_vals) * up_vals).astype(jnp.bfloat16)
    hidden_width = whole_down.shape[1]
    group_width = hidden_width // tp_count
    expert_sum = jnp.zeros(arrived.shape[:3] + (model_width,), jnp.float32)
    for index in range(tp_count):
        piece = jnp.einsum(
            "secf,efd->secd",
            expert_hidden[..., index * group_width : (index + 1) * group_width],
            whole_down[:, index * group_width : (index + 1) * group_width, :],
            preferred_element_type=jnp.float32,
        )
        expert_sum = expert_sum + piece.astype(jnp.bfloat16).astype(jnp.float32)
    expert_rows = expert_sum.astype(jnp.bfloat16)
    back = lax.all_to_all(expert_rows, SP, split_axis=0, concat_axis=0, tiled=True)
    back_flat = back.reshape(sp_count * group_count * capacity, model_width)
    owner_sp = flat_routes // local_experts
    local_slot = flat_routes % local_experts - tp_index * group_count
    belongs = (local_slot >= 0) & (local_slot < group_count)
    local_position = jnp.where(
        belongs, (owner_sp * group_count + local_slot) * capacity + slot_index, 0
    )
    picked = jnp.take(back_flat, local_position, axis=0).reshape(
        tokens_here, top_count, model_width
    )
    kept_weight = jnp.where(belongs.reshape(tokens_here, top_count), router_weight_matrix, 0.0)
    routed_partial = jnp.sum(kept_weight[:, :, None] * picked.astype(jnp.float32), axis=1)
    shared_rounded = shared_partial.astype(jnp.bfloat16).astype(jnp.float32)
    combined = summed_on_arrival((routed_partial + shared_rounded).astype(jnp.bfloat16), "tp", 1)
    return (stream_share + combined).astype(jnp.bfloat16)


def solution(mesh):
    split = Mesh(mesh.devices.reshape(8, 4, 2, mesh.shape["tp"]), ("sp_0", "sp_1", "sp_2", "tp"))
    return jax.shard_map(
        body,
        mesh=split,
        in_specs=(
            P(SP, "tp"),
            P(SP, "tp"),
            P(SP, "tp"),
            P(SP, "tp"),
            P("tp", SP),
            P("tp", SP),
            P("tp"),
            P("tp", SP),
            P("tp"),
            P(),
            P(SP, None),
            P(),
            P(SP, None),
            P(SP, None),
            P(SP, None, "tp"),
            P(SP, None, "tp"),
            P(SP, "tp", None),
            P(None, "tp"),
            P(None, "tp"),
            P("tp", None),
        ),
        out_specs=P(SP, "tp"),
        check_vma=False,
    )
```

profile of v0, /device:TPU:1, one launch (start us, length us, event | category | flops | bytes accessed | tf_op | source)
XLA Modules:
  0.0 357.7 jit_solution(7305421903418140099)
XLA Ops:
  0.0 4.6 %pad_maximum_fusion = bf16[4,4096,128]{2,1,0:T(8,128)(2,1)} fusion(bf16[4,2048,128]{2,1,0:T(8,128)(2,1)} %param.35, bf16[4,2048,128]{2,1,0:T(8,128)(2,1)} %param.34), kind=kLoop, calls=%fused_computation.5 | loop fusion | flops 8388608 | bytes 8388608 | tf_op jit(solution)/shard_map/concatenate | solution.py:57
  4.7 5.0 %all-to-all-start = ((bf16[4,4096,128]{2,1,0:T(8,128)(2,1)}), bf16[4,4096,128]{2,1,0:T(8,128)(2,1)}, u32[]{:S(2)}, u32[]{:S(2)}) async-start(bf16[4,4096,128]{2,1,0:T(8,128)(2,1)} %pad_maximum_fusion), calls=%async_computation | async-start | bytes 8388608 | tf_op jit(solution)/shard_map/all_to_all | solution.py:60
  12.6 4.8 %all-gather.3 = f32[2,194,96]{1,2,0:T(8,128)S(1)} all-gather(f32[1,194,96]{1,2,0:T(8,128)S(1)} %maximum_bitcast_fusion), channel_id=2, replica_groups=mesh['sp_0'=8,'sp_1'=4,'sp_2'=2,'tp'=4] {'sp_2'}, dimensions={0}, use_global_device_ids=true | all-gather | bytes 223488 | tf_op jit(solution)/shard_map/all_gather | solution.py:28
  19.1 10.8 %all-gather.4 = f32[4,194,96]{1,2,0:T(8,128)S(1)} all-gather(f32[1,194,96]{1,2,0:T(8,128)S(1)} %maximum_bitcast_fusion.1), channel_id=3, replica_groups=mesh['sp_0'=8,'sp_1'=4,'sp_2'=2,'tp'=4] {'sp_1'}, dimensions={0}, use_global_device_ids=true | all-gather | bytes 372480 | tf_op jit(solution)/shard_map/all_gather | solution.py:28
  52.5 1.4 copy.129
  53.8 1.4 copy.128
  56.9 23.1 %all-gather.5 = f32[8,194,96]{1,2,0:T(8,128)S(1)} all-gather(f32[1,194,96]{1,2,0:T(8,128)S(1)} %maximum_bitcast_fusion.2), channel_id=4, replica_groups=mesh['sp_0'=8,'sp_1'=4,'sp_2'=2,'tp'=4] {'sp_0'}, dimensions={0}, use_global_device_ids=true | all-gather | bytes 670464 | tf_op jit(solution)/shard_map/all_gather | solution.py:28
  86.4 1.7 fusion.37
  88.0 1.6 squeeze.170
  89.7 1.6 squeeze.171
  91.3 1.6 squeeze.172
  93.0 1.6 squeeze.173
  94.6 1.6 squeeze.174
  96.3 1.7 squeeze.175
  97.9 1.6 squeeze.176
  99.6 1.6 squeeze.177
  101.2 1.6 squeeze.178
  102.9 1.7 squeeze.179
  106.0 1.6 squeeze.182
  107.7 1.6 squeeze.183
  113.4 4.3 %scatter_custom_fusion = s32[2048]{0:T(1024)S(1)} fusion(s32[1024]{0:T(1024)S(1)} %bitcast.491, s32[1024]{0:T(1024)S(1)} %add_select_fusion.4, s32[]{:T(128)} %constant.144.clone.1), kind=kCustom, calls=%fused_computation.266 | custom fusion | bytes 8196 | tf_op jit(solution)/shard_map/scatter | solution.py:188
  123.3 2.2 fusion.28
  125.5 2.3 multiply_reduce_fusion.2
  128.0 10.4 %all_gather.27 = bf16[256,768]{0,1:T(8,128)(2,1)S(1)} all-gather(bf16[256,192]{0,1:T(8,128)(2,1)S(1)} %fusion.46), channel_id=1, replica_groups=mesh['sp_0'=8,'sp_1'=4,'sp_2'=2,'tp'=4] {'tp'}, dimensions={1}, use_global_device_ids=true | all-gather | bytes 491520 | tf_op jit(solution)/shard_map/all_gather | solution.py:161
  140.9 3.3 gather_fusion
  144.3 1.8 fusion.8
  146.1 68.0 %all_to_all.45 = bf16[64,1,8,2048]{3,2,1,0:T(8,128)(2,1)} all-to-all(bf16[64,1,8,2048]{3,2,1,0:T(8,128)(2,1)S(1)} %fusion.8), channel_id=1, replica_groups=mesh['sp_0'=8,'sp_1'=4,'sp_2'=2,'tp'=4] {'sp_0','sp_1','sp_2'}, dimensions={0} | all-to-all | bytes 4194304 | tf_op jit(solution)/shard_map/all_to_all | solution.py:205
  214.1 3.6 %all-to-all-start.2 = ((bf16[4,128,2048]{2,1,0:T(8,128)(2,1)}), bf16[4,128,2048]{2,1,0:T(8,128)(2,1)S(1)}, u32[]{:S(2)}, u32[]{:S(2)}) async-start(bf16[4,128,2048]{2,1,0:T(8,128)(2,1)} %param.36), calls=%async_computation.2 | async-start | bytes 4194304 | tf_op jit(solution)/shard_map/all_to_all | solution.py:199
  217.7 2.8 copy_bitcast_fusion
  220.6 1.3 fusion.11
  221.9 1.5 fusion.20
  224.3 17.8 %all-to-all-done.2 = bf16[4,128,2048]{2,1,0:T(8,128)(2,1)S(1)} async-done(((bf16[4,128,2048]{2,1,0:T(8,128)(2,1)}), bf16[4,128,2048]{2,1,0:T(8,128)(2,1)S(1)}, u32[]{:S(2)}, u32[]{:S(2)}) %all-to-all-start.2) | async-done | bytes 2097184 | tf_op jit(solution)/shard_map/all_to_all | solution.py:199
  242.0 1.3 copy-done.3
  243.4 1.9 convolution_convert_fusion.1
  246.8 2.5 fusion
  249.3 9.2 %all-to-all-start.3 = ((bf16[64,1,8,2048]{3,2,1,0:T(8,128)(2,1)}), bf16[64,1,8,2048]{3,2,1,0:T(8,128)(2,1)S(1)}, u32[]{:S(2)}, u32[]{:S(2)}) async-start(bf16[64,1,8,2048]{3,2,1,0:T(8,128)(2,1)} %fusion), calls=%async_computation.3 | async-start | bytes 4194304 | tf_op jit(solution)/shard_map/all_to_all | solution.py:223
  259.7 1.6 compare_and_fusion
  262.1 1.5 fusion.233
  263.5 44.7 %all-to-all-done.3 = bf16[64,1,8,2048]{3,2,1,0:T(8,128)(2,1)S(1)} async-done(((bf16[64,1,8,2048]{3,2,1,0:T(8,128)(2,1)}), bf16[64,1,8,2048]{3,2,1,0:T(8,128)(2,1)S(1)}, u32[]{:S(2)}, u32[]{:S(2)}) %all-to-all-start.3) | async-done | bytes 2097184 | tf_op jit(solution)/shard_map/all_to_all | solution.py:223
  308.3 6.1 %gather_fusion.1 = bf16[1024,2048]{1,0:T(8,128)(2,1)} fusion(bf16[512,2048]{1,0:T(8,128)(2,1)S(1)} %bitcast.465, s32[1024]{0:T(1024)S(1)} %broadcast_clamp_fusion), kind=kCustom, calls=%fused_computation.1 | custom fusion | bytes 8392704 | tf_op jit(solution)/shard_map/jit(_take)/gather | solution.py:231
  314.3 7.2 %gather.15 = bf16[256,4,2048]{2,1,0:T(4,128)(2,1)} reshape(bf16[1024,2048]{1,0:T(8,128)(2,1)} %gather_fusion.1) | data formatting | bytes 8388608 | tf_op jit(solution)/shard_map/jit(_take)/gather | solution.py:231
  321.5 9.9 %multiply_reduce_fusion = f32[256,2048]{1,0:T(8,128)S(1)} fusion(bf16[256,4,2048]{2,1,0:T(4,128)(2,1)} %gather.15, f32[256,4]{1,0:T(8,128)S(1)} %fusion.67, pred[256,4]{1,0:T(8,128)(4,1)S(1)} %copy-done.14), kind=kLoop, calls=%fused_computation.3 | loop fusion | flops 7864320 | bytes 6296576 | tf_op jit(solution)/shard_map/reduce_sum | solution.py:235
  331.5 3.0 fusion.3
  334.5 2.3 copy.353
  336.8 4.5 %all-to-all-start.4 = ((bf16[4,256,512]{2,1,0:T(8,128)(2,1)}), bf16[4,256,512]{2,1,0:T(8,128)(2,1)}, u32[]{:S(2)}, u32[]{:S(2)}) async-start(bf16[4,256,512]{2,1,0:T(8,128)(2,1)} %bitcast.470), calls=%async_computation.4 | async-start | bytes 2097152 | tf_op jit(solution)/shard_map/all_to_all | solution.py:75
  341.3 13.2 %all-to-all-done.4 = bf16[4,256,512]{2,1,0:T(8,128)(2,1)} async-done(((bf16[4,256,512]{2,1,0:T(8,128)(2,1)}), bf16[4,256,512]{2,1,0:T(8,128)(2,1)}, u32[]{:S(2)}, u32[]{:S(2)}) %all-to-all-start.4) | async-done | bytes 1048608 | tf_op jit(solution)/shard_map/all_to_all | solution.py:75
  354.5 1.4 convert_reduce_fusion
  355.9 1.8 add_convert_fusion.1
  (197 shorter events, 52.9 us)
Async XLA Ops:
  0.0 138.4 %copy-start = (bf16[768,2048]{1,0:T(8,128)(2,1)S(1)}, bf16[768,2048]{1,0:T(8,128)(2,1)}, u32[]{:S(2)}) copy-start(bf16[768,2048]{1,0:T(8,128)(2,1)} %param.29) | copy-start | bytes 9437188
  4.6 5.7 %copy-start.34 = (f32[2,256]{1,0:T(2,128)S(1)}, f32[2,256]{1,0:T(2,128)}, u32[]{:S(2)}) copy-start(f32[2,256]{1,0:T(2,128)} %param.27) | copy-start | bytes 6148
  4.6 5.7 %copy-start.35 = (f32[2,256]{1,0:T(2,128)S(1)}, f32[2,256]{1,0:T(2,128)}, u32[]{:S(2)}) copy-start(f32[2,256]{1,0:T(2,128)} %param.25) | copy-start | bytes 6148
  4.6 5.7 %copy-start.41 = (f32[2]{0:T(128)S(1)}, f32[2]{0:T(128)}, u32[]{:S(2)}) copy-start(f32[2]{0:T(128)} %param.26) | copy-start | bytes 28
  4.6 7.1 %copy-start.25 = (f32[2,256]{1,0:T(2,128)S(1)}, f32[2,256]{1,0:T(2,128)}, u32[]{:S(2)}) copy-start(f32[2,256]{1,0:T(2,128)} %param.24) | copy-start | bytes 6148
  4.6 7.3 %copy-start.15 = (bf16[256,192]{0,1:T(8,128)(2,1)S(1)}, bf16[256,192]{0,1:T(8,128)(2,1)}, u32[]{:S(2)}) copy-start(bf16[256,192]{0,1:T(8,128)(2,1)} %param.22) | copy-start | bytes 294916
  4.6 7.3 %copy-start.16 = (bf16[256,192]{0,1:T(8,128)(2,1)S(1)}, bf16[256,192]{0,1:T(8,128)(2,1)}, u32[]{:S(2)}) copy-start(bf16[256,192]{0,1:T(8,128)(2,1)} %param.21) | copy-start | bytes 294916
  4.7 141.4 %all-to-all-start = ((bf16[4,4096,128]{2,1,0:T(8,128)(2,1)}), bf16[4,4096,128]{2,1,0:T(8,128)(2,1)}, u32[]{:S(2)}, u32[]{:S(2)}) async-start(bf16[4,4096,128]{2,1,0:T(8,128)(2,1)} %pad_maximum_fusion), calls=%async_computation | async-start | bytes 8388608 | tf_op jit(solution)/shard_map/all_to_all | solution.py:60
  11.5 74.9 %copy-start.19 = (f32[1,2,2,128]{3,1,2,0:T(2,128)}, f32[1,2,2,128]{3,1,2,0:T(2,128)S(1)}, u32[]{:S(2)}) copy-start(f32[1,2,2,128]{3,1,2,0:T(2,128)S(1)} %copy.354) | copy-start | bytes 6148
  17.4 1.6 copy-start.6
  17.7 1.1 copy-start.23
  17.7 0.9 copy-start.37
  17.7 1.1 copy-start.26
  17.7 1.1 copy-start.27
  17.8 0.5 copy-start.40
  17.8 0.7 copy-start.39
  17.8 1.0 copy-start.33
  17.8 1.3 copy-start.38
  30.3 51.7 %copy-start.18 = (f32[4,96]{1,0:T(4,128)}, f32[4,96]{1,0:T(4,128)S(1)}, u32[]{:S(2)}) copy-start(f32[4,96]{1,0:T(4,128)S(1)} %get-tuple-element.6) | copy-start | bytes 4612
  30.9 1.2 copy-start.28
  30.9 1.2 copy-start.29
  30.9 1.2 copy-start.30
  30.9 1.3 copy-start.31
  32.1 0.5 copy-start.42
  79.9 2.9 copy-start.7
  79.9 3.6 %copy-start.20 = (s32[256,4]{0,1:T(4,128)S(1)}, s32[256,4]{0,1:T(4,128)}, u32[]{:S(2)}) copy-start(s32[256,4]{0,1:T(4,128)} %param.32) | copy-start | bytes 12292
  82.9 21.7 %copy-start.12 = (f32[1,192,96]{1,2,0:T(8,128)S(1)}, f32[1,192,96]{1,2,0:T(8,128)}, u32[]{:S(2)}) copy-start(f32[1,192,96]{1,2,0:T(8,128)} %get-tuple-element.52) | copy-start | bytes 221188
  82.9 22.4 %copy-start.11 = (f32[1,192,96]{1,2,0:T(8,128)S(1)}, f32[1,192,96]{1,2,0:T(8,128)}, u32[]{:S(2)}) copy-start(f32[1,192,96]{1,2,0:T(8,128)} %get-tuple-element.54) | copy-start | bytes 221188
  109.6 1.1 copy-start.5
  112.0 11.3 %copy-start.13 = (pred[256,256]{1,0:T(8,128)(4,1)S(1)}, pred[256,256]{1,0:T(8,128)(4,1)}, u32[]{:S(2)}) copy-start(pred[256,256]{1,0:T(8,128)(4,1)} %iota_compare_fusion.3) | copy-start | bytes 196612
  123.3 4.6 %copy-start.17 = (bf16[256,192]{0,1:T(8,128)(2,1)S(1)}, bf16[256,192]{0,1:T(8,128)(2,1)}, u32[]{:S(2)}) copy-start(bf16[256,192]{0,1:T(8,128)(2,1)} %param.23) | copy-start | bytes 294916
  123.3 4.6 %copy-start.36 = (f32[192]{0:T(256)S(1)}, f32[192]{0:T(256)}, u32[]{:S(2)}) copy-start(f32[192]{0:T(256)} %param.28) | copy-start | bytes 2308
  125.5 12.9 %copy-start.9 = (bf16[256,2048]{1,0:T(8,128)(2,1)S(1)}, bf16[256,2048]{1,0:T(8,128)(2,1)}, u32[]{:S(2)}) copy-start(bf16[256,2048]{1,0:T(8,128)(2,1)} %param.30) | copy-start | bytes 3145732
  138.4 1.1 copy-start.24
  139.5 1.4 copy-start.2
  214.1 27.9 %all-to-all-start.2 = ((bf16[4,128,2048]{2,1,0:T(8,128)(2,1)}), bf16[4,128,2048]{2,1,0:T(8,128)(2,1)S(1)}, u32[]{:S(2)}, u32[]{:S(2)}) async-start(bf16[4,128,2048]{2,1,0:T(8,128)(2,1)} %param.36), calls=%async_computation.2 | async-start | bytes 4194304 | tf_op jit(solution)/shard_map/all_to_all | solution.py:199
  217.7 2.9 copy-start.8
  242.0 1.3 copy-start.3
  242.0 3.3 copy-start.10
  243.4 2.0 copy-start.4
  249.3 9.4 %copy-start.21 = (s32[256,4]{0,1:T(4,128)S(1)}, s32[256,4]{0,1:T(4,128)}, u32[]{:S(2)}) copy-start(s32[256,4]{0,1:T(4,128)} %param.32) | copy-start | bytes 12292
  249.3 10.2 %copy-start.32 = (f32[256,4]{0,1:T(4,128)S(1)}, f32[256,4]{0,1:T(4,128)}, u32[]{:S(2)}) copy-start(f32[256,4]{0,1:T(4,128)} %param.33) | copy-start | bytes 12292
  249.3 10.3 %copy-start.22 = (s32[1024,1]{0,1:T(1,128)S(1)}, s32[1024,1]{0,1:T(1,128)}, u32[]{:S(2)}) copy-start(s32[1024,1]{0,1:T(1,128)} %get-tuple-element.57) | copy-start | bytes 12292
  249.3 59.0 %all-to-all-start.3 = ((bf16[64,1,8,2048]{3,2,1,0:T(8,128)(2,1)}), bf16[64,1,8,2048]{3,2,1,0:T(8,128)(2,1)S(1)}, u32[]{:S(2)}, u32[]{:S(2)}) async-start(bf16[64,1,8,2048]{3,2,1,0:T(8,128)(2,1)} %fusion), calls=%async_computation.3 | async-start | bytes 4194304 | tf_op jit(solution)/shard_map/all_to_all | solution.py:223
  314.3 7.2 %copy-start.14 = (pred[256,4]{1,0:T(8,128)(4,1)S(1)}, pred[256,4]{1,0:T(8,128)(4,1)}, u32[]{:S(2)}) copy-start(pred[256,4]{1,0:T(8,128)(4,1)} %compare_and_fusion) | copy-start | bytes 3076
  336.8 21.0 %copy-start.1 = (bf16[768,2048]{1,0:T(8,128)(2,1)S(1)}, bf16[768,2048]{1,0:T(8,128)(2,1)}, u32[]{:S(2)}) copy-start(bf16[768,2048]{1,0:T(8,128)(2,1)} %param.29) | copy-start | bytes 9437188
  336.8 17.7 %all-to-all-start.4 = ((bf16[4,256,512]{2,1,0:T(8,128)(2,1)}), bf16[4,256,512]{2,1,0:T(8,128)(2,1)}, u32[]{:S(2)}, u32[]{:S(2)}) async-start(bf16[4,256,512]{2,1,0:T(8,128)(2,1)} %bitcast.470), calls=%async_computation.4 | async-start | bytes 2097152 | tf_op jit(solution)/shard_map/all_to_all | solution.py:75
where the time goes:
time: 361 us; the launch traced here: 358 us
  blocking collectives  117 us (32%)
  local copies, waits for them, and re-layouts  87.4 us (24%)
  waiting for transfers between devices  75.7 us (21%)
  other arithmetic  35.4 us (10%)
  starting transfers between devices  22.4 us (6%)
  matrix products  19 us (5%)
    all_to_all x1, blocking collectives, body(): lax.all_to_all(outgoing, SP, split_axis=0, concat_axis=0, tiled=True)  68 us
    all_to_all x1, waiting for transfers between devices, body(): lax.all_to_all(expert_rows, SP, split_axis=0, concat_axis=0, tiled=True)  44.7 us
    all_gather x3, blocking collectives, gathered_once(): both, at, found = (lax.all_gather(jnp.concatenate(lines), axis), 0, {})  38.7 us
    squeeze x14, local copies, waits for them, and re-layouts, entering(): subtotal = combine(subtotal, jax.tree.map(lambda part: part[k], pieces))  21.3 us
    all_to_all x1, waiting for transfers between devices, body(): lax.all_to_all(routed_down_weight, 'tp', split_axis=0, concat_axis=1, til...  17.8 us
    gather x2, local copies, waits for them, and re-layouts, body(): jnp.take(back_flat, local_position, axis=0)  13.3 us
    all_to_all x1, waiting for transfers between devices, summed_on_arrival(): lax.all_to_all(cut_along(shard, dim, count), axis, 0, 0, tiled=True)  13.2 us
    all_gather x1, blocking collectives, body(): lax.all_gather(token_mixing, 'tp', axis=1, tiled=True)  10.4 us
  transfers between devices with their start and end apart: 4, of which 3 were waited for; matrix products, arithmetic and copies ran while one was open for 27% of the time, Pallas kernels for 0%

commit v1 on v0

v1 whole, which is shorter than its diff:
```python
import jax
import jax.numpy as jnp
from jax import lax
from jax.experimental import pallas as pl
from jax.experimental.pallas import tpu as pltpu
from jax.sharding import Mesh
from jax.sharding import PartitionSpec as P

SP = ("sp_0", "sp_1", "sp_2")
MESH_ID = pl.DeviceIdType.MESH
NEG_LARGE = -1e30
EPSILON = 1e-06
F32 = jnp.float32
BF16 = jnp.bfloat16
HIGHEST = lax.Precision.HIGHEST

NZ, NY, NC, NX = 8, 4, 2, 4
PLANE = NY * NC
N_SP = NZ * PLANE
TOK = 256
DH = 96
HW = 192
D = 2048
FF = 512
GROUP = FF // NX
CAP = 8
SLOTS = N_SP * CAP
NEAR = PLANE * NX * CAP
LANES = 128
SLICE = HW // PLANE
QUARTER = D // NX
CHUNK = 2 * PLANE


def nt(a, b, precision=None):
    return lax.dot_general(
        a, b, (((1,), (1,)), ((), ())), preferred_element_type=F32, precision=precision
    )


def tn(a, b, precision=None):
    return lax.dot_general(
        a, b, (((0,), (0,)), ((), ())), preferred_element_type=F32, precision=precision
    )


def nn(a, b, precision=None):
    return jnp.dot(a, b, preferred_element_type=F32, precision=precision)


def arrival(ref, sem):
    pltpu.make_async_copy(ref, ref, sem).wait()


def z_offset(i):
    return jnp.where(lax.rem(i, 2) == 0, 4 + i // 2, 4 - (i + 1) // 2)


def kernel(
    q_hbm,
    k_hbm,
    v_hbm,
    og_hbm,
    lig_hbm,
    fpre_hbm,
    bias_ref,
    boost_hbm,
    hgain_ref,
    wo_hbm,
    res_hbm,
    egain_ref,
    routes_hbm,
    rw_hbm,
    gate_hbm,
    up_hbm,
    down_hbm,
    sg_hbm,
    su_hbm,
    sd_hbm,
    out_ref,
    q_ref,
    k_ref,
    v_ref,
    og_ref,
    lig_ref,
    fpre_ref,
    boost_ref,
    wo_ref,
    res_ref,
    routes_ref,
    rw_ref,
    sg_ref,
    su_ref,
    sd_ref,
    wg_ref,
    wu_ref,
    wd_ref,
    state_ref,
    plane_ref,
    zst_ref,
    fin_ref,
    carry_ref,
    mix_ref,
    mixed_ref,
    hidden_ref,
    stream_ref,
    normed_ref,
    pick_ref,
    whi_ref,
    wlo_ref,
    shared_ref,
    sbuf_ref,
    rbuf_ref,
    eo_ref,
    near_ref,
    rs_ref,
    chain_out_ref,
    chain_in_ref,
    table_ref,
    in_sem,
    own_sem,
    wsend_sem,
    wrecv_sem,
    st_send,
    st_recv,
    mix_send,
    mix_recv,
    d_send,
    d_recv,
    b_send,
    b_recv,
    rs_ssem,
    rs_rsem,
    chain_send,
    chain_recv,
):
    z, y, c, x = (lax.axis_index(a) for a in ("sp_0", "sp_1", "sp_2", "tp"))
    p = y * NC + c
    sp = z * PLANE + p

    def sp_dev(tz, tp_):
        return {"sp_0": tz, "sp_1": tp_ // NC, "sp_2": lax.rem(tp_, NC)}

    early = (
        (lig_hbm, lig_ref),
        (fpre_hbm, fpre_ref),
        (boost_hbm, boost_ref),
        (k_hbm, k_ref),
        (v_hbm, v_ref),
        (q_hbm, q_ref),
        (og_hbm, og_ref),
        (routes_hbm, routes_ref),
        (rw_hbm, rw_ref),
        (wo_hbm, wo_ref),
        (res_hbm, res_ref),
        (sg_hbm, sg_ref),
        (su_hbm, su_ref),
        (sd_hbm, sd_ref),
    )
    loads = [pltpu.make_async_copy(a, b, in_sem.at[n]) for n, (a, b) in enumerate(early)]
    for cp in loads:
        cp.start()

    barrier = pltpu.get_barrier_semaphore()

    @pl.loop(1, N_SP)
    def _(n):
        pl.semaphore_signal(
            barrier,
            inc=1,
            device_id=sp_dev(lax.rem(z + n // PLANE, NZ), lax.rem(p + n, PLANE)),
            device_id_type=MESH_ID,
        )

    @pl.loop(0, (NX - 1) * PLANE)
    def _(n):
        pl.semaphore_signal(
            barrier,
            inc=1,
            device_id={
                **sp_dev(z, lax.rem(p + n, PLANE)),
                "tp": lax.rem(x + 1 + n // PLANE, NX),
            },
            device_id_type=MESH_ID,
        )

    own_weights = (
        pltpu.make_async_copy(
            gate_hbm.at[x], wg_ref.at[:, pl.ds(pl.multiple_of(x * GROUP, GROUP), GROUP)], own_sem.at[0]
        ),
        pltpu.make_async_copy(
            up_hbm.at[x], wu_ref.at[:, pl.ds(pl.multiple_of(x * GROUP, GROUP), GROUP)], own_sem.at[1]
        ),
        pltpu.make_async_copy(
            down_hbm.at[x], wd_ref.at[pl.ds(pl.multiple_of(x * GROUP, GROUP), GROUP)], own_sem.at[2]
        ),
    )

    for n in range(3):
        loads[n].wait()
    second = lax.broadcasted_iota(jnp.int32, (2, TOK), 0) == 1
    bias = jnp.where(second, bias_ref[1], bias_ref[0])
    pre = fpre_ref[...] + bias
    log_forget = jnp.minimum(pre, 0.0) - jnp.log1p(jnp.exp(-jnp.abs(pre))) + boost_ref[...]
    row = lax.broadcasted_iota(jnp.int32, (TOK, TOK), 0)
    col = lax.broadcasted_iota(jnp.int32, (TOK, TOK), 1)
    causal = row <= col
    upper = jnp.where(causal, 1.0, 0.0).astype(F32)
    eye = jnp.where(row == col, 1.0, 0.0).astype(F32)
    log_in = lig_ref[...]
    cumul = nn(log_forget, upper, HIGHEST)
    source = nt(eye, log_in - cumul, HIGHEST)
    ending = jnp.sum(log_forget, axis=1, keepdims=True)
    w_log = ending - cumul + log_in
    local_top = jnp.max(w_log, axis=1, keepdims=True)
    w_end = jnp.exp(w_log - local_top)

    loads[3].wait()
    loads[4].wait()
    lane = lax.broadcasted_iota(jnp.int32, (DH, LANES), 1)
    slice_lane = lax.broadcasted_iota(jnp.int32, (SLICE, LANES), 1)

    def with_scalars(mem, top, total, lanes):
        return jnp.where(lanes == DH, top, jnp.where(lanes == DH + 1, total, mem))

    def taken_apart(block):
        return block, block[:, DH : DH + 1], block[:, DH + 1 : DH + 2]

    padding = jnp.zeros((LANES - DH, TOK), F32)
    for h in range(2):
        keys = k_ref[h * DH : (h + 1) * DH].astype(F32) * w_end[h : h + 1]
        values = v_ref[h * DH : (h + 1) * DH].astype(F32)
        memory = nt(values, jnp.concatenate([keys, padding], axis=0), HIGHEST)
        state = with_scalars(memory, local_top[h : h + 1], ending[h : h + 1], lane)
        state_ref[h * (PLANE // 2) : (h + 1) * (PLANE // 2)] = state.reshape(PLANE // 2, SLICE, LANES)

    pl.semaphore_wait(barrier, N_SP - 1 + (NX - 1) * PLANE)

    @pl.loop(1, PLANE)
    def _(n):
        to = lax.rem(p + n, PLANE)
        pltpu.make_async_remote_copy(
            state_ref.at[to],
            plane_ref.at[p],
            st_send.at[0],
            st_recv.at[0],
            device_id=sp_dev(z, to),
            device_id_type=MESH_ID,
        ).start()

    own_rows = pl.ds(pl.multiple_of(x * GROUP, GROUP), GROUP)

    def send_weights(n, src, dst):
        for step in (1, 3, 2):
            to = lax.rem(x + step, NX)
            pltpu.make_async_remote_copy(
                src(to),
                dst,
                wsend_sem.at[n],
                wrecv_sem.at[n],
                device_id={"tp": to},
                device_id_type=MESH_ID,
            ).start()

    upper_half, lower_half = pl.ds(0, D // 2), pl.ds(D // 2, D // 2)
    send_weights(0, lambda to: gate_hbm.at[to, upper_half], wg_ref.at[upper_half, own_rows])
    for cp in own_weights:
        cp.start()
    plane_ref[p] = state_ref[p]

    loads[5].wait()
    scale = DH ** (-0.5)
    local_max, numer = [], []
    for h in range(2):
        head = slice(h * DH, (h + 1) * DH)
        d_log = jnp.where(causal, cumul[h : h + 1] + source[:, h : h + 1], NEG_LARGE)
        top = jnp.max(d_log, axis=0, keepdims=True)
        scores = tn(k_ref[head], q_ref[head]) * scale
        within = (scores * jnp.exp(d_log - top)).astype(BF16)
        numer.append(nn(v_ref[head], within))
        local_max.append(top)

    def join(earlier, later):
        mem_a, top_a, total_a = earlier
        mem_b, top_b, total_b = later
        top = jnp.maximum(total_b + top_a, top_b)
        mem = jnp.exp(total_b + top_a - top) * mem_a + jnp.exp(top_b - top) * mem_b
        return mem, top, total_a + total_b

    none = (
        jnp.zeros((SLICE, LANES), F32),
        jnp.full((SLICE, 1), NEG_LARGE, F32),
        jnp.zeros((SLICE, 1), F32),
    )
    arrival(plane_ref.at[pl.ds(0, PLANE - 1)], st_recv.at[0])
    whole, before = none, []
    for n in range(PLANE):
        before.append(whole)
        whole = join(whole, taken_apart(plane_ref[n]))
    zst_ref[z] = with_scalars(*whole, slice_lane)

    @pl.loop(1, NZ)
    def _(n):
        pltpu.make_async_remote_copy(
            zst_ref.at[z],
            zst_ref.at[z],
            st_send.at[1],
            st_recv.at[1],
            device_id={"sp_0": lax.rem(z + n, NZ)},
            device_id_type=MESH_ID,
        ).start()

    loads[7].wait()
    loads[8].wait()
    table_ref[z] = jnp.concatenate([routes_ref[...].astype(F32), rw_ref[...]], axis=0)

    @pl.loop(1, NZ)
    def _(n):
        pltpu.make_async_remote_copy(
            table_ref.at[z],
            table_ref.at[z],
            st_send.at[3],
            st_recv.at[3],
            device_id={"sp_0": lax.rem(z + n, NZ)},
            device_id_type=MESH_ID,
        ).start()

    slot = lax.broadcasted_iota(jnp.int32, (SLOTS, TOK), 0)
    expert = slot // CAP * NX + x
    named = jnp.zeros((SLOTS, TOK), F32)
    for n in range(4):
        named = jnp.where(routes_ref[n : n + 1] == expert, 1.0, named)
    strict = jnp.where(row < col, 1.0, 0.0).astype(BF16)
    rank = nn(named.astype(BF16), strict)
    pick_ref[...] = jnp.where(rank == lax.rem(slot, CAP).astype(F32), named, 0.0).astype(BF16)
    hgain = nt(eye[:HW, :HW], hgain_ref[...], HIGHEST)
    loads[6].wait()
    gating = hgain * jax.nn.sigmoid(og_ref[...].astype(F32))

    arrival(zst_ref.at[pl.ds(0, NZ - 1)], st_recv.at[1])
    carried = none
    for n in range(NZ):
        mem, top, total = taken_apart(zst_ref[n])
        passed = n < z
        carried = join(
            carried, (mem, jnp.where(passed, top, NEG_LARGE), jnp.where(passed, total, 0.0))
        )
    z_mem, z_top, z_total = carried
    z_mem = jnp.where(z > 0, z_mem, 0.0)
    for n in range(PLANE):
        fin_ref[n] = with_scalars(*join((z_mem, z_top, z_total), before[n]), slice_lane)

    @pl.loop(1, PLANE)
    def _(n):
        to = lax.rem(p + n, PLANE)
        pltpu.make_async_remote_copy(
            fin_ref.at[to],
            carry_ref.at[p],
            st_send.at[2],
            st_recv.at[2],
            device_id=sp_dev(z, to),
            device_id_type=MESH_ID,
        ).start()

    carry_ref[p] = fin_ref[p]
    arrival(carry_ref.at[pl.ds(0, PLANE - 1)], st_recv.at[2])
    no_queries = jnp.zeros((LANES - DH, TOK), BF16)
    for h in range(2):
        head = slice(h * DH, (h + 1) * DH)
        memory = carry_ref[h * (PLANE // 2) : (h + 1) * (PLANE // 2)].reshape(DH, LANES)
        carry_top = memory[0:1, DH : DH + 1]
        memory = jnp.where(lane < DH, memory, 0.0)
        high = memory.astype(BF16)
        low = (memory - high.astype(F32)).astype(BF16)
        queries = jnp.concatenate([q_ref[head], no_queries], axis=0)
        inter = nn(high, queries) + nn(low, queries)
        g_log = cumul[h : h + 1] + carry_top
        stab = jnp.maximum(g_log, local_max[h])
        cell = numer[h] * jnp.exp(local_max[h] - stab) + inter * (jnp.exp(g_log - stab) * scale)
        mean = jnp.sum(cell * cell, axis=0, keepdims=True) / DH
        mix_ref[x, head] = (cell * lax.rsqrt(mean + EPSILON) * gating[head]).astype(BF16)
    for step in (1, 3, 2):
        pltpu.make_async_remote_copy(
            mix_ref.at[x],
            mix_ref.at[x],
            mix_send,
            mix_recv,
            device_id={"tp": lax.rem(x + step, NX)},
            device_id_type=MESH_ID,
        ).start()
    send_weights(0, lambda to: gate_hbm.at[to, lower_half], wg_ref.at[lower_half, own_rows])
    send_weights(1, lambda to: up_hbm.at[to], wu_ref.at[:, own_rows])
    send_weights(2, lambda to: down_hbm.at[to], wd_ref.at[own_rows])

    loads[9].wait()
    loads[10].wait()
    arrival(mix_ref.at[pl.ds(0, NX - 1)], mix_recv)
    mixed_ref[...] = jnp.transpose(mix_ref[...].astype(F32).reshape(NX * HW, TOK)).astype(BF16)

    def project(n, total):
        columns = pl.ds(pl.multiple_of(n * QUARTER, QUARTER), QUARTER)
        part = res_ref[:, columns].astype(F32) + nn(mixed_ref[...], wo_ref[:, columns])
        stream_ref[n] = part
        return total + jnp.sum(part * part, axis=1, keepdims=True)

    square = lax.fori_loop(0, NX, project, jnp.zeros((TOK, 1), F32))
    inverse = lax.rsqrt(square / D + EPSILON)

    @pl.loop(0, NX)
    def _(n):
        columns = pl.ds(pl.multiple_of(n * QUARTER, QUARTER), QUARTER)
        normed_ref[:, columns] = (stream_ref[n] * inverse * egain_ref[:, columns]).astype(BF16)

    @pl.loop(0, NZ)
    def _(i):
        to_z = lax.rem(z + z_offset(i), NZ)
        chosen = pick_ref[pl.ds(pl.multiple_of(to_z * PLANE * CAP, PLANE * CAP), PLANE * CAP)]
        rows = nn(chosen, normed_ref[...])
        sbuf_ref[pl.ds(i * PLANE, PLANE)] = rows.reshape(PLANE, CAP, D).astype(BF16)

        @pl.loop(0, PLANE)
        def _(n):
            to = lax.rem(p + n, PLANE)
            itself = (i == NZ - 1) & (n == 0)

            @pl.when(jnp.logical_not(itself))
            def _():
                pltpu.make_async_remote_copy(
                    sbuf_ref.at[i * PLANE + to],
                    rbuf_ref.at[i * PLANE + p],
                    d_send,
                    d_recv.at[i],
                    device_id=sp_dev(to_z, to),
                    device_id_type=MESH_ID,
                ).start()

            @pl.when(itself)
            def _():
                pltpu.make_async_copy(
                    sbuf_ref.at[i * PLANE + to], rbuf_ref.at[i * PLANE + p], d_recv.at[i]
                ).start()

    for n in range(11, 14):
        loads[n].wait()
    normed = normed_ref[...]
    shared_hidden = (jax.nn.silu(nn(normed, sg_ref[...])) * nn(normed, su_ref[...])).astype(BF16)
    for n in range(NX):
        shared_ref[n] = nn(shared_hidden, sd_ref[:, n * QUARTER : (n + 1) * QUARTER]).astype(BF16)

    arrival(table_ref.at[pl.ds(0, NZ - 1)], st_recv.at[3])
    slot = lax.broadcasted_iota(jnp.int32, (NEAR, TOK), 0)
    expert = (slot // CAP + z * (PLANE * NX)).astype(F32)
    place = lax.rem(slot, CAP).astype(F32)

    @pl.loop(0, NZ)
    def _(n):
        table = table_ref[n]
        named = jnp.zeros((NEAR, TOK), F32)
        weight = jnp.zeros((NEAR, TOK), F32)
        for k in range(4):
            hit = table[k : k + 1] == expert
            named = jnp.where(hit, 1.0, named)
            weight = jnp.where(hit, table[k + 4 : k + 5], weight)
        rank = nn(named.astype(BF16), strict)
        weight = jnp.transpose(jnp.where(rank == place, weight, 0.0))
        high = weight.astype(BF16)
        whi_ref[n] = high
        wlo_ref[n] = (weight - high.astype(F32)).astype(BF16)

    for cp in own_weights:
        cp.wait()
    arrival(wg_ref.at[:, pl.ds(0, FF - GROUP)], wrecv_sem.at[0])
    arrival(wu_ref.at[:, pl.ds(0, FF - GROUP)], wrecv_sem.at[1])

    @pl.loop(0, NZ // 2)
    def _(s):
        arrival(rbuf_ref.at[pl.ds(0, PLANE)], d_recv.at[2 * s])
        arrival(rbuf_ref.at[pl.ds(0, PLANE)], d_recv.at[2 * s + 1])
        blocks = pl.ds(pl.multiple_of(s * CHUNK, CHUNK), CHUNK)
        rows = rbuf_ref[blocks].astype(F32).reshape(CHUNK * CAP, D).astype(BF16)
        hidden = jax.nn.silu(nn(rows, wg_ref[...])) * nn(rows, wu_ref[...])
        hidden_ref[s] = hidden.astype(BF16)

    arrival(wd_ref.at[pl.ds(0, FF - GROUP)], wrecv_sem.at[2])

    @pl.loop(0, NZ // 2)
    def _(s):
        for n in range(NX):
            result = nn(hidden_ref[s], wd_ref[:, n * QUARTER : (n + 1) * QUARTER])
            result = result.reshape(2, PLANE, CAP, QUARTER).astype(BF16)
            for k in range(2):
                eo_ref[s, n, :, k] = result[k]

        @pl.loop(0, NX * PLANE)
        def _(n):
            to, to_x = lax.rem(p + n // NX, PLANE), lax.rem(x + n, NX)

            @pl.when(n > 0)
            def _():
                pltpu.make_async_remote_copy(
                    eo_ref.at[s, to_x, to],
                    near_ref.at[s, p * NX + x],
                    b_send,
                    b_recv.at[s],
                    device_id={**sp_dev(z, to), "tp": to_x},
                    device_id_type=MESH_ID,
                ).start()

            @pl.when(n == 0)
            def _():
                pltpu.make_async_copy(
                    eo_ref.at[s, to_x, to], near_ref.at[s, p * NX + x], b_recv.at[s]
                ).start()

    for step in (1, 3, 2):
        to = lax.rem(x + step, NX)
        pltpu.make_async_remote_copy(
            shared_ref.at[to],
            rs_ref.at[x],
            rs_ssem,
            rs_rsem,
            device_id={"tp": to},
            device_id_type=MESH_ID,
        ).start()

    width = QUARTER // 2

    def weighted(i, h):
        block = lax.rem(z + NZ - z_offset(i), NZ)
        rows = near_ref[i // 2, :, i % 2, :, h * width : (h + 1) * width]
        rows = rows.astype(F32).reshape(NEAR, width).astype(BF16)
        return nn(whi_ref[block], rows) + nn(wlo_ref[block], rows)

    def arrived(i, h):
        arrival(chain_in_ref.at[2 * i + h], chain_recv.at[2 * i + h])
        return chain_in_ref[2 * i + h].astype(F32)

    def passed_on(i, h, before, up):
        part = weighted(i, h)
        if before is not None:
            part = part + arrived(before, h)
        chain_out_ref[2 * i + h] = part.astype(BF16)
        pltpu.make_async_remote_copy(
            chain_out_ref.at[2 * i + h],
            chain_in_ref.at[2 * i + h],
            chain_send,
            chain_recv.at[2 * i + h],
            device_id={"sp_0": lax.rem(z + (1 if up else NZ - 1), NZ)},
            device_id_type=MESH_ID,
        ).start()

    arrival(near_ref.at[0], b_recv.at[0])
    passed_on(0, 0, None, True)
    passed_on(0, 1, None, False)
    passed_on(1, 0, None, False)
    arrival(near_ref.at[1], b_recv.at[1])
    passed_on(2, 1, None, True)
    passed_on(1, 1, 0, False)
    passed_on(2, 0, 0, True)
    passed_on(3, 0, 1, False)
    arrival(near_ref.at[2], b_recv.at[2])
    passed_on(4, 1, 2, True)
    passed_on(3, 1, 1, False)
    passed_on(4, 0, 2, True)
    passed_on(5, 0, 3, False)
    arrival(near_ref.at[3], b_recv.at[3])
    passed_on(6, 1, 4, True)
    passed_on(5, 1, 3, False)
    passed_on(6, 0, 4, True)

    rs_ref[x] = shared_ref[x]
    arrival(rs_ref.at[pl.ds(0, NX - 1)], rs_rsem)
    totals = []
    for h in range(2):
        columns = slice(h * width, (h + 1) * width)
        total = stream_ref[x, :, columns] + weighted(NZ - 1, h)
        for n in range(NX):
            total = total + rs_ref[n, :, columns].astype(F32)
        totals.append(total)
    for h in range(2):
        total = totals[h] + arrived(5, h) + arrived(6, h)
        out_ref[:, h * width : (h + 1) * width] = total.astype(BF16)

    arrival(plane_ref.at[pl.ds(0, PLANE - 1)], st_send.at[0])
    arrival(zst_ref.at[pl.ds(0, NZ - 1)], st_send.at[1])
    arrival(fin_ref.at[pl.ds(0, PLANE - 1)], st_send.at[2])
    arrival(mix_ref.at[pl.ds(0, NX - 1)], mix_send)
    arrival(wg_ref.at[:, pl.ds(0, FF - GROUP)], wsend_sem.at[0])
    arrival(wu_ref.at[:, pl.ds(0, FF - GROUP)], wsend_sem.at[1])
    arrival(wd_ref.at[pl.ds(0, FF - GROUP)], wsend_sem.at[2])
    arrival(sbuf_ref.at[pl.ds(0, N_SP - 1)], d_send)
    arrival(table_ref.at[pl.ds(0, NZ - 1)], st_send.at[3])
    for n in range(NZ // 2):
        arrival(near_ref.at[n, pl.ds(0, NX * PLANE - 1)], b_send)
    arrival(rs_ref.at[pl.ds(0, NX - 1)], rs_ssem)
    arrival(chain_out_ref, chain_send)


def body(
    memory_queries,
    memory_keys,
    memory_values,
    output_gate_preactivation,
    log_input_gate,
    forget_preactivation,
    head_forget_bias,
    forget_extra_boost,
    head_norm_gain,
    memory_output_weight,
    residual,
    expert_norm_gain,
    routes,
    router_weight_matrix,
    routed_gate_weight,
    routed_up_weight,
    routed_down_weight,
    shared_gate_weight,
    shared_up_weight,
    shared_down_weight,
):
    anywhere = pl.BlockSpec(memory_space=pl.ANY)
    vmem = pl.BlockSpec(memory_space=pltpu.VMEM)
    smem = pl.BlockSpec(memory_space=pltpu.SMEM)
    specs = [anywhere] * 20
    specs[6] = smem
    specs[8] = vmem
    specs[11] = vmem
    dma = pltpu.SemaphoreType.DMA
    return pl.pallas_call(
        kernel,
        out_shape=jax.ShapeDtypeStruct((TOK, QUARTER), BF16),
        in_specs=specs,
        out_specs=vmem,
        scratch_shapes=[
            pltpu.VMEM((HW, TOK), BF16),
            pltpu.VMEM((HW, TOK), BF16),
            pltpu.VMEM((HW, TOK), BF16),
            pltpu.VMEM((HW, TOK), BF16),
            pltpu.VMEM((2, TOK), F32),
            pltpu.VMEM((2, TOK), F32),
            pltpu.VMEM((2, TOK), F32),
            pltpu.VMEM((NX * HW, D), BF16),
            pltpu.VMEM((TOK, D), BF16),
            pltpu.VMEM((4, TOK), jnp.int32),
            pltpu.VMEM((4, TOK), F32),
            pltpu.VMEM((D, GROUP), BF16),
            pltpu.VMEM((D, GROUP), BF16),
            pltpu.VMEM((GROUP, D), BF16),
            pltpu.VMEM((D, FF), BF16),
            pltpu.VMEM((D, FF), BF16),
            pltpu.VMEM((FF, D), BF16),
            pltpu.VMEM((PLANE, SLICE, LANES), F32),
            pltpu.VMEM((PLANE, SLICE, LANES), F32),
            pltpu.VMEM((NZ, SLICE, LANES), F32),
            pltpu.VMEM((PLANE, SLICE, LANES), F32),
            pltpu.VMEM((PLANE, SLICE, LANES), F32),
            pltpu.VMEM((NX, HW, TOK), BF16),
            pltpu.VMEM((TOK, NX * HW), BF16),
            pltpu.VMEM((NZ // 2, CHUNK * CAP, FF), BF16),
            pltpu.VMEM((NX, TOK, QUARTER), F32),
            pltpu.VMEM((TOK, D), BF16),
            pltpu.VMEM((SLOTS, TOK), BF16),
            pltpu.VMEM((NZ, TOK, NEAR), BF16),
            pltpu.VMEM((NZ, TOK, NEAR), BF16),
            pltpu.VMEM((NX, TOK, QUARTER), BF16),
            pltpu.VMEM((N_SP, CAP, D), BF16),
            pltpu.VMEM((N_SP, CAP, D), BF16),
            pltpu.VMEM((NZ // 2, NX, PLANE, 2, CAP, QUARTER), BF16),
            pltpu.VMEM((NZ // 2, NX * PLANE, 2, CAP, QUARTER), BF16),
            pltpu.VMEM((NX, TOK, QUARTER), BF16),
            pltpu.VMEM((14, TOK, QUARTER // 2), BF16),
            pltpu.VMEM((14, TOK, QUARTER // 2), BF16),
            pltpu.VMEM((NZ, 8, TOK), F32),
            dma((14,)),
            dma((3,)),
            dma((3,)),
            dma((3,)),
            dma((4,)),
            dma((4,)),
            dma,
            dma,
            dma,
            dma((NZ,)),
            dma,
            dma((NZ // 2,)),
            dma,
            dma,
            dma,
            dma((14,)),
        ],
        compiler_params=pltpu.CompilerParams(
            collective_id=0, has_side_effects=True, vmem_limit_bytes=60 << 20
        ),
        name="layer",
    )(
        memory_queries.T,
        memory_keys.T,
        memory_values.T,
        output_gate_preactivation.T,
        log_input_gate,
        forget_preactivation,
        head_forget_bias,
        forget_extra_boost,
        head_norm_gain.reshape(1, HW),
        memory_output_weight,
        residual,
        expert_norm_gain.reshape(1, D),
        routes.T,
        router_weight_matrix.T,
        routed_gate_weight,
        routed_up_weight,
        routed_down_weight,
        shared_gate_weight,
        shared_up_weight,
        shared_down_weight,
    )


def solution(mesh):
    split = Mesh(
        mesh.devices.reshape(NZ, NY, NC, mesh.shape["tp"]), ("sp_0", "sp_1", "sp_2", "tp")
    )
    return jax.shard_map(
        body,
        mesh=split,
        in_specs=(
            P(SP, "tp"),
            P(SP, "tp"),
            P(SP, "tp"),
            P(SP, "tp"),
            P("tp", SP),
            P("tp", SP),
            P("tp"),
            P("tp", SP),
            P("tp"),
            P(),
            P(SP, None),
            P(),
            P(SP, None),
            P(SP, None),
            P(SP, None, "tp"),
            P(SP, None, "tp"),
            P(SP, "tp", None),
            P(None, "tp"),
            P(None, "tp"),
            P("tp", None),
        ),
        out_specs=P(SP, "tp"),
        check_vma=False,
    )
```

time: 361 us -> 131 us (0.36)
  Pallas kernels: 0 us -> 129 us
  blocking collectives: 117 us -> 0 us
  local copies, waits for them, and re-layouts: 87.4 us -> 1.67 us
  waiting for transfers between devices: 75.7 us -> 0 us
  other arithmetic: 35.4 us -> 0 us
  starting transfers between devices: 22.4 us -> 0 us
  matrix products: 19 us -> 0 us
    pallas_call x0 -> x1, Pallas kernels: none -> 129 us  [body(): pl.pallas_call(kernel, out_shape=jax.ShapeDtypeStruct((TOK, QUARTER), BF1...]
    all_to_all x4 -> x0, waiting for transfers between devices: 75.7 us -> none  [the longest x1 44.7 us: body(): lax.all_to_all(expert_rows, SP, split_axis=0, concat_axis=0, tiled=True)]
    all_to_all x1 -> x0, blocking collectives: 68 us -> none  [body(): lax.all_to_all(outgoing, SP, split_axis=0, concat_axis=0, tiled=True)]
    all_gather x4 -> x0, blocking collectives: 49.1 us -> none  [the longest x3 38.7 us: gathered_once(): both, at, found = (lax.all_gather(jnp.concatenate(lines), axis), 0, {})]
    all_to_all x4 -> x0, starting transfers between devices: 22.4 us -> none  [the longest x1 9.25 us: body(): lax.all_to_all(expert_rows, SP, split_axis=0, concat_axis=0, tiled=True)]
    squeeze x14 -> x0, local copies, waits for them, and re-layouts: 21.3 us -> none  [entering(): subtotal = combine(subtotal, jax.tree.map(lambda part: part[k], pieces))]
    mul x24 -> x0, local copies, waits for them, and re-layouts: 19.3 us -> none  [the longest x12 10.2 us: join_states(): own_weight[:, None, None] * memory_b]
    dot_general x12 -> x0, matrix products: 19 us -> none  [the longest x4 5.9 us: body(): jnp.einsum('secf,efd->secd', expert_hidden[..., index * group_width:(inde...]
  transfers between devices with their start and end apart: 4 -> 0, of which waited for: 3 -> 0; matrix products, arithmetic and copies ran while one was open for 27% -> 0% of each run, Pallas kernels for 0% -> 0%
where the time goes in v1:
time: 131 us
  Pallas kernels  129 us (98%)
  local copies, waits for them, and re-layouts  1.67 us (1%)
    pallas_call x1, Pallas kernels, body(): pl.pallas_call(kernel, out_shape=jax.ShapeDtypeStruct((TOK, QUARTER), BF1...  129 us

profile of v1, /device:TPU:1, one launch (start us, length us, event | category | flops | bytes accessed | tf_op | source)
XLA Modules:
  0.0 130.6 jit_solution(16461908590336183925)
XLA Ops:
  0.0 128.9 %layer.1 = bf16[256,512]{1,0:T(8,128)(2,1)} custom-call(bf16[192,256]{1,0:T(8,128)(2,1)} %bitcast.8, bf16[192,256]{1,0:T(8,128)(2,1)} %bitcast.9, bf16[192,256]{1,0:T(8,128)(2,1)} %bitcast.10, bf16[192,256]{1,0:T(8,128)(2,1)} %bitcast.11, f32[2,256]{1,0:T(2,128)} %lig_hbm.1, f32[2,256]{1,0:T(2,128)} %fpre_hbm.1, f32[2]{0:T(128)} %bias_ref.1, ...), custom_call_target="tpu_custom_call" | custom-call | tf_op jit(solution)/shard_map/layer/pallas_call | solution.py:629
  128.9 1.7 %copy.22 = bf16[256,512]{1,0:T(8,128)(2,1)} copy(bf16[256,512]{1,0:T(8,128)(2,1)} %layer.1) | data formatting | bytes 524288

commit v2 on v1

--- a/solution.py
+++ b/solution.py
@@ -27,6 +27,7 @@
 SLOTS = N_SP * CAP
 NEAR = PLANE * NX * CAP
 LANES = 128
+SOON = 1024
 SLICE = HW // PLANE
 QUARTER = D // NX
 CHUNK = 2 * PLANE
@@ -113,7 +114,6 @@
     rbuf_ref,
     eo_ref,
     near_ref,
-    rs_ref,
     chain_out_ref,
     chain_in_ref,
     table_ref,
@@ -133,6 +133,8 @@
     rs_rsem,
     chain_send,
     chain_recv,
+    swap_send,
+    swap_recv,
 ):
     z, y, c, x = (lax.axis_index(a) for a in ("sp_0", "sp_1", "sp_2", "tp"))
     p = y * NC + c
@@ -140,6 +142,11 @@
 
     def sp_dev(tz, tp_):
         return {"sp_0": tz, "sp_1": tp_ // NC, "sp_2": lax.rem(tp_, NC)}
+
+    own_rows = pl.ds(pl.multiple_of(x * GROUP, GROUP), GROUP)
+
+    def quarter_of(n):
+        return pl.ds(pl.multiple_of(n * QUARTER, QUARTER), QUARTER)
 
     early = (
         (lig_hbm, lig_ref),
@@ -155,7 +162,7 @@
         (res_hbm, res_ref),
         (sg_hbm, sg_ref),
         (su_hbm, su_ref),
-        (sd_hbm, sd_ref),
+        (sd_hbm.at[:, quarter_of(x)], sd_ref.at[own_rows]),
     )
     loads = [pltpu.make_async_copy(a, b, in_sem.at[n]) for n, (a, b) in enumerate(early)]
     for cp in loads:
@@ -163,36 +170,33 @@
 
     barrier = pltpu.get_barrier_semaphore()
 
-    @pl.loop(1, N_SP)
+    @pl.loop(1, NZ)
     def _(n):
         pl.semaphore_signal(
-            barrier,
-            inc=1,
-            device_id=sp_dev(lax.rem(z + n // PLANE, NZ), lax.rem(p + n, PLANE)),
-            device_id_type=MESH_ID,
+            barrier, inc=1, device_id={"sp_0": lax.rem(z + n, NZ)}, device_id_type=MESH_ID
         )
 
-    @pl.loop(0, (NX - 1) * PLANE)
+    @pl.loop(1, NX * PLANE)
     def _(n):
         pl.semaphore_signal(
             barrier,
             inc=1,
             device_id={
                 **sp_dev(z, lax.rem(p + n, PLANE)),
-                "tp": lax.rem(x + 1 + n // PLANE, NX),
+                "tp": lax.rem(x + n // PLANE, NX),
             },
             device_id_type=MESH_ID,
         )
 
     own_weights = (
         pltpu.make_async_copy(
-            gate_hbm.at[x], wg_ref.at[:, pl.ds(pl.multiple_of(x * GROUP, GROUP), GROUP)], own_sem.at[0]
+            gate_hbm.at[x], wg_ref.at[:, own_rows], own_sem.at[0]
         ),
         pltpu.make_async_copy(
-            up_hbm.at[x], wu_ref.at[:, pl.ds(pl.multiple_of(x * GROUP, GROUP), GROUP)], own_sem.at[1]
+            up_hbm.at[x], wu_ref.at[:, own_rows], own_sem.at[1]
         ),
         pltpu.make_async_copy(
-            down_hbm.at[x], wd_ref.at[pl.ds(pl.multiple_of(x * GROUP, GROUP), GROUP)], own_sem.at[2]
+            down_hbm.at[x], wd_ref.at[own_rows], own_sem.at[2]
         ),
     )
 
@@ -234,7 +238,7 @@
         state = with_scalars(memory, local_top[h : h + 1], ending[h : h + 1], lane)
         state_ref[h * (PLANE // 2) : (h + 1) * (PLANE // 2)] = state.reshape(PLANE // 2, SLICE, LANES)
 
-    pl.semaphore_wait(barrier, N_SP - 1 + (NX - 1) * PLANE)
+    pl.semaphore_wait(barrier, NZ - 1 + NX * PLANE - 1)
 
     @pl.loop(1, PLANE)
     def _(n):
@@ -248,10 +252,8 @@
             device_id_type=MESH_ID,
         ).start()
 
-    own_rows = pl.ds(pl.multiple_of(x * GROUP, GROUP), GROUP)
-
     def send_weights(n, src, dst):
-        for step in (1, 3, 2):
+        for step in (2, 1, 3):
             to = lax.rem(x + step, NX)
             pltpu.make_async_remote_copy(
                 src(to),
@@ -262,7 +264,19 @@
                 device_id_type=MESH_ID,
             ).start()
 
-    upper_half, lower_half = pl.ds(0, D // 2), pl.ds(D // 2, D // 2)
+    upper_half, lower_half = pl.ds(0, SOON), pl.ds(SOON, D - SOON)
+    def core_rows(k):
+        start = pl.multiple_of(k * GROUP + c * (GROUP // NC), GROUP // NC)
+        return pl.ds(start, GROUP // NC)
+
+    send_weights(
+        3,
+        lambda to: sd_hbm.at[
+            pl.ds(pl.multiple_of(c * (GROUP // NC), GROUP // NC), GROUP // NC),
+            quarter_of(to),
+        ],
+        sd_ref.at[core_rows(x)],
+    )
     send_weights(0, lambda to: gate_hbm.at[to, upper_half], wg_ref.at[upper_half, own_rows])
     for cp in own_weights:
         cp.start()
@@ -390,7 +404,18 @@
         ).start()
     send_weights(0, lambda to: gate_hbm.at[to, lower_half], wg_ref.at[lower_half, own_rows])
     send_weights(1, lambda to: up_hbm.at[to], wu_ref.at[:, own_rows])
-    send_weights(2, lambda to: down_hbm.at[to], wd_ref.at[own_rows])
+    for j in (0, 1, 3, 2):
+        for step in (2, 1, 3):
+            to = lax.rem(x + step, NX)
+            columns = quarter_of(lax.rem(to + j, NX))
+            pltpu.make_async_remote_copy(
+                down_hbm.at[to, :, columns],
+                wd_ref.at[own_rows, columns],
+                wsend_sem.at[2],
+                wrecv_sem.at[4 if j == 2 else 2],
+                device_id={"tp": to},
+                device_id_type=MESH_ID,
+            ).start()
 
     loads[9].wait()
     loads[10].wait()
@@ -398,7 +423,7 @@
     mixed_ref[...] = jnp.transpose(mix_ref[...].astype(F32).reshape(NX * HW, TOK)).astype(BF16)
 
     def project(n, total):
-        columns = pl.ds(pl.multiple_of(n * QUARTER, QUARTER), QUARTER)
+        columns = quarter_of(n)
         part = res_ref[:, columns].astype(F32) + nn(mixed_ref[...], wo_ref[:, columns])
         stream_ref[n] = part
         return total + jnp.sum(part * part, axis=1, keepdims=True)
@@ -408,7 +433,7 @@
 
     @pl.loop(0, NX)
     def _(n):
-        columns = pl.ds(pl.multiple_of(n * QUARTER, QUARTER), QUARTER)
+        columns = quarter_of(n)
         normed_ref[:, columns] = (stream_ref[n] * inverse * egain_ref[:, columns]).astype(BF16)
 
     @pl.loop(0, NZ)
@@ -440,12 +465,22 @@
                     sbuf_ref.at[i * PLANE + to], rbuf_ref.at[i * PLANE + p], d_recv.at[i]
                 ).start()
 
+    arrival(sd_ref.at[pl.ds(0, (NX - 1) * (GROUP // NC))], wrecv_sem.at[3])
+    for step in range(1, NX):
+        rows = core_rows(lax.rem(x + step, NX))
+        pltpu.make_async_remote_copy(
+            sd_ref.at[rows],
+            sd_ref.at[rows],
+            swap_send,
+            swap_recv,
+            device_id={"sp_2": 1 - c},
+            device_id_type=MESH_ID,
+        ).start()
     for n in range(11, 14):
         loads[n].wait()
     normed = normed_ref[...]
-    shared_hidden = (jax.nn.silu(nn(normed, sg_ref[...])) * nn(normed, su_ref[...])).astype(BF16)
-    for n in range(NX):
-        shared_ref[n] = nn(shared_hidden, sd_ref[:, n * QUARTER : (n + 1) * QUARTER]).astype(BF16)
+    shared_hidden = jax.nn.silu(nn(normed, sg_ref[...])) * nn(normed, su_ref[...])
+    shared_ref[:, own_rows] = shared_hidden.astype(BF16)
 
     arrival(table_ref.at[pl.ds(0, NZ - 1)], st_recv.at[3])
     slot = lax.broadcasted_iota(jnp.int32, (NEAR, TOK), 0)
@@ -481,47 +516,54 @@
         hidden = jax.nn.silu(nn(rows, wg_ref[...])) * nn(rows, wu_ref[...])
         hidden_ref[s] = hidden.astype(BF16)
 
-    arrival(wd_ref.at[pl.ds(0, FF - GROUP)], wrecv_sem.at[2])
-
-    @pl.loop(0, NZ // 2)
-    def _(s):
-        for n in range(NX):
-            result = nn(hidden_ref[s], wd_ref[:, n * QUARTER : (n + 1) * QUARTER])
-            result = result.reshape(2, PLANE, CAP, QUARTER).astype(BF16)
-            for k in range(2):
-                eo_ref[s, n, :, k] = result[k]
-
-        @pl.loop(0, NX * PLANE)
-        def _(n):
-            to, to_x = lax.rem(p + n // NX, PLANE), lax.rem(x + n, NX)
-
-            @pl.when(n > 0)
-            def _():
+    arrival(wd_ref.at[pl.ds(0, FF - GROUP), pl.ds(0, D - QUARTER)], wrecv_sem.at[2])
+
+    def send_back(src, dst, sem, columns):
+        for j in columns:
+            to_x = lax.rem(x + j, NX)
+
+            @pl.loop(0 if j else 1, PLANE)
+            def _(n):
+                to = lax.rem(p + n, PLANE)
                 pltpu.make_async_remote_copy(
-                    eo_ref.at[s, to_x, to],
-                    near_ref.at[s, p * NX + x],
+                    src(to_x, to),
+                    dst,
                     b_send,
-                    b_recv.at[s],
+                    sem,
                     device_id={**sp_dev(z, to), "tp": to_x},
                     device_id_type=MESH_ID,
                 ).start()
 
-            @pl.when(n == 0)
-            def _():
-                pltpu.make_async_copy(
-                    eo_ref.at[s, to_x, to], near_ref.at[s, p * NX + x], b_recv.at[s]
-                ).start()
-
-    for step in (1, 3, 2):
-        to = lax.rem(x + step, NX)
-        pltpu.make_async_remote_copy(
-            shared_ref.at[to],
-            rs_ref.at[x],
-            rs_ssem,
-            rs_rsem,
-            device_id={"tp": to},
-            device_id_type=MESH_ID,
-        ).start()
+            if j == 0:
+                pltpu.make_async_copy(src(x, p), dst, sem).start()
+
+    def out_of_expert(s, k, rows, columns):
+        for j in columns:
+            n = lax.rem(x + j, NX)
+            result = nn(rows, wd_ref[:, quarter_of(n)])
+            result = result.reshape(-1, PLANE, CAP, QUARTER).astype(BF16)
+            for m in range(result.shape[0]):
+                eo_ref[s, n, :, k + m] = result[m]
+
+    def both_back(s, columns):
+        out_of_expert(s, 0, hidden_ref[s], columns)
+        send_back(
+            lambda to_x, to: eo_ref.at[s, to_x, to],
+            near_ref.at[s, p * NX + x],
+            b_recv.at[2 * s],
+            columns,
+        )
+
+    def one_back(i, columns):
+        s, k = i // 2, i % 2
+        rows = hidden_ref[s, k * (PLANE * CAP) : (k + 1) * (PLANE * CAP)]
+        out_of_expert(s, k, rows, columns)
+        send_back(
+            lambda to_x, to: eo_ref.at[s, to_x, to, k],
+            near_ref.at[s, p * NX + x, k],
+            b_recv.at[i],
+            columns,
+        )
 
     width = QUARTER // 2
 
@@ -549,37 +591,56 @@
             device_id_type=MESH_ID,
         ).start()
 
-    arrival(near_ref.at[0], b_recv.at[0])
+    soon, every = (1, 3, 0), (2, 1, 3, 0)
+    one_back(0, soon)
+    one_back(1, soon)
+    arrival(wd_ref.at[pl.ds(0, FF - GROUP), pl.ds(0, QUARTER)], wrecv_sem.at[4])
+    one_back(0, (2,))
+    one_back(1, (2,))
+    both_back(1, every)
+    both_back(2, every)
+    arrival(near_ref.at[0, :, 0], b_recv.at[0])
     passed_on(0, 0, None, True)
     passed_on(0, 1, None, False)
+    arrival(near_ref.at[0, :, 1], b_recv.at[1])
     passed_on(1, 0, None, False)
-    arrival(near_ref.at[1], b_recv.at[1])
+    one_back(6, every)
+    arrival(near_ref.at[1], b_recv.at[2])
     passed_on(2, 1, None, True)
+    passed_on(2, 0, 0, True)
     passed_on(1, 1, 0, False)
-    passed_on(2, 0, 0, True)
+    one_back(7, every)
+    for step in (2, 1, 3):
+        pltpu.make_async_remote_copy(
+            shared_ref.at[:, own_rows],
+            shared_ref.at[:, own_rows],
+            rs_ssem,
+            rs_rsem,
+            device_id={"tp": lax.rem(x + step, NX)},
+            device_id_type=MESH_ID,
+        ).start()
     passed_on(3, 0, 1, False)
-    arrival(near_ref.at[2], b_recv.at[2])
+    arrival(near_ref.at[2], b_recv.at[4])
     passed_on(4, 1, 2, True)
     passed_on(3, 1, 1, False)
     passed_on(4, 0, 2, True)
     passed_on(5, 0, 3, False)
-    arrival(near_ref.at[3], b_recv.at[3])
+    arrival(near_ref.at[3, :, 0], b_recv.at[6])
     passed_on(6, 1, 4, True)
     passed_on(5, 1, 3, False)
     passed_on(6, 0, 4, True)
 
-    rs_ref[x] = shared_ref[x]
-    arrival(rs_ref.at[pl.ds(0, NX - 1)], rs_rsem)
+    arrival(near_ref.at[3, :, 1], b_recv.at[7])
     totals = []
     for h in range(2):
+        totals.append(stream_ref[x, :, h * width : (h + 1) * width] + weighted(NZ - 1, h))
+    arrival(sd_ref.at[pl.ds(0, (NX - 1) * (GROUP // NC))], swap_recv)
+    arrival(shared_ref.at[:, pl.ds(0, FF - GROUP)], rs_rsem)
+    for h in range(2):
         columns = slice(h * width, (h + 1) * width)
-        total = stream_ref[x, :, columns] + weighted(NZ - 1, h)
-        for n in range(NX):
-            total = total + rs_ref[n, :, columns].astype(F32)
-        totals.append(total)
-    for h in range(2):
-        total = totals[h] + arrived(5, h) + arrived(6, h)
-        out_ref[:, h * width : (h + 1) * width] = total.astype(BF16)
+        total = totals[h] + nn(shared_ref[...], sd_ref[:, columns])
+        total = total + arrived(5, h) + arrived(6, h)
+        out_ref[:, columns] = total.astype(BF16)
 
     arrival(plane_ref.at[pl.ds(0, PLANE - 1)], st_send.at[0])
     arrival(zst_ref.at[pl.ds(0, NZ - 1)], st_send.at[1])
@@ -592,7 +653,9 @@
     arrival(table_ref.at[pl.ds(0, NZ - 1)], st_send.at[3])
     for n in range(NZ // 2):
         arrival(near_ref.at[n, pl.ds(0, NX * PLANE - 1)], b_send)
-    arrival(rs_ref.at[pl.ds(0, NX - 1)], rs_ssem)
+    arrival(sd_ref.at[pl.ds(0, (NX - 1) * (GROUP // NC))], wsend_sem.at[3])
+    arrival(sd_ref.at[pl.ds(0, (NX - 1) * (GROUP // NC))], swap_send)
+    arrival(shared_ref.at[:, pl.ds(0, FF - GROUP)], rs_ssem)
     arrival(chain_out_ref, chain_send)
 
 
@@ -645,7 +708,7 @@
             pltpu.VMEM((4, TOK), F32),
             pltpu.VMEM((D, GROUP), BF16),
             pltpu.VMEM((D, GROUP), BF16),
-            pltpu.VMEM((GROUP, D), BF16),
+            pltpu.VMEM((FF, QUARTER), BF16),
             pltpu.VMEM((D, FF), BF16),
             pltpu.VMEM((D, FF), BF16),
             pltpu.VMEM((FF, D), BF16),
@@ -662,19 +725,18 @@
             pltpu.VMEM((SLOTS, TOK), BF16),
             pltpu.VMEM((NZ, TOK, NEAR), BF16),
             pltpu.VMEM((NZ, TOK, NEAR), BF16),
-            pltpu.VMEM((NX, TOK, QUARTER), BF16),
+            pltpu.VMEM((TOK, FF), BF16),
             pltpu.VMEM((N_SP, CAP, D), BF16),
             pltpu.VMEM((N_SP, CAP, D), BF16),
             pltpu.VMEM((NZ // 2, NX, PLANE, 2, CAP, QUARTER), BF16),
             pltpu.VMEM((NZ // 2, NX * PLANE, 2, CAP, QUARTER), BF16),
-            pltpu.VMEM((NX, TOK, QUARTER), BF16),
             pltpu.VMEM((14, TOK, QUARTER // 2), BF16),
             pltpu.VMEM((14, TOK, QUARTER // 2), BF16),
             pltpu.VMEM((NZ, 8, TOK), F32),
             dma((14,)),
             dma((3,)),
-            dma((3,)),
-            dma((3,)),
+            dma((4,)),
+            dma((5,)),
             dma((4,)),
             dma((4,)),
             dma,
@@ -682,11 +744,13 @@
             dma,
             dma((NZ,)),
             dma,
-            dma((NZ // 2,)),
+            dma((NZ,)),
             dma,
             dma,
             dma,
             dma((14,)),
+            dma,
+            dma,
         ],
         compiler_params=pltpu.CompilerParams(
             collective_id=0, has_side_effects=True, vmem_limit_bytes=60 << 20

time: 131 us -> 125 us (0.954)
  Pallas kernels: 129 us -> 123 us
    pallas_call x1, Pallas kernels: 129 us -> 123 us  [body(): pl.pallas_call(kernel, out_shape=jax.ShapeDtypeStruct((TOK, QUARTER), BF1...]
where the time goes in v2:
time: 125 us
  Pallas kernels  123 us (98%)
  local copies, waits for them, and re-layouts  1.67 us (1%)
    pallas_call x1, Pallas kernels, body(): pl.pallas_call(kernel, out_shape=jax.ShapeDtypeStruct((TOK, QUARTER), BF1...  123 us

profile of v2, /device:TPU:1, one launch (start us, length us, event | category | flops | bytes accessed | tf_op | source)
XLA Modules:
  0.0 124.6 jit_solution(3358429843510593039)
XLA Ops:
  0.0 122.9 %layer.1 = bf16[256,512]{1,0:T(8,128)(2,1)} custom-call(bf16[192,256]{1,0:T(8,128)(2,1)} %bitcast.8, bf16[192,256]{1,0:T(8,128)(2,1)} %bitcast.9, bf16[192,256]{1,0:T(8,128)(2,1)} %bitcast.10, bf16[192,256]{1,0:T(8,128)(2,1)} %bitcast.11, f32[2,256]{1,0:T(2,128)} %lig_hbm.1, f32[2,256]{1,0:T(2,128)} %fpre_hbm.1, f32[2]{0:T(128)} %bias_ref.1, ...), custom_call_target="tpu_custom_call" | custom-call | tf_op jit(solution)/shard_map/layer/pallas_call | solution.py:692
  122.9 1.7 %copy.22 = bf16[256,512]{1,0:T(8,128)(2,1)} copy(bf16[256,512]{1,0:T(8,128)(2,1)} %layer.1) | data formatting | bytes 524288

commit v3 on v2

--- a/solution.py
+++ b/solution.py
@@ -23,11 +23,12 @@
 D = 2048
 FF = 512
 GROUP = FF // NX
+PART = GROUP // PLANE
 CAP = 8
 SLOTS = N_SP * CAP
 NEAR = PLANE * NX * CAP
 LANES = 128
-SOON = 1024
+SOON = 1280
 SLICE = HW // PLANE
 QUARTER = D // NX
 CHUNK = 2 * PLANE
@@ -176,16 +177,15 @@
             barrier, inc=1, device_id={"sp_0": lax.rem(z + n, NZ)}, device_id_type=MESH_ID
         )
 
-    @pl.loop(1, NX * PLANE)
+    @pl.loop(1, PLANE)
     def _(n):
         pl.semaphore_signal(
-            barrier,
-            inc=1,
-            device_id={
-                **sp_dev(z, lax.rem(p + n, PLANE)),
-                "tp": lax.rem(x + n // PLANE, NX),
-            },
-            device_id_type=MESH_ID,
+            barrier, inc=1, device_id=sp_dev(z, lax.rem(p + n, PLANE)), device_id_type=MESH_ID
+        )
+
+    for n in range(1, NX):
+        pl.semaphore_signal(
+            barrier, inc=1, device_id={"tp": lax.rem(x + n, NX)}, device_id_type=MESH_ID
         )
 
     own_weights = (
@@ -238,7 +238,7 @@
         state = with_scalars(memory, local_top[h : h + 1], ending[h : h + 1], lane)
         state_ref[h * (PLANE // 2) : (h + 1) * (PLANE // 2)] = state.reshape(PLANE // 2, SLICE, LANES)
 
-    pl.semaphore_wait(barrier, NZ - 1 + NX * PLANE - 1)
+    pl.semaphore_wait(barrier, NZ - 1 + PLANE - 1 + NX - 1)
 
     @pl.loop(1, PLANE)
     def _(n):
@@ -265,17 +265,16 @@
             ).start()
 
     upper_half, lower_half = pl.ds(0, SOON), pl.ds(SOON, D - SOON)
-    def core_rows(k):
-        start = pl.multiple_of(k * GROUP + c * (GROUP // NC), GROUP // NC)
-        return pl.ds(start, GROUP // NC)
+    def part_rows(k):
+        return pl.ds(pl.multiple_of(k * GROUP + p * PART, PART), PART)
 
     send_weights(
         3,
         lambda to: sd_hbm.at[
-            pl.ds(pl.multiple_of(c * (GROUP // NC), GROUP // NC), GROUP // NC),
+            pl.ds(pl.multiple_of(p * PART, PART), PART),
             quarter_of(to),
         ],
-        sd_ref.at[core_rows(x)],
+        sd_ref.at[part_rows(x)],
     )
     send_weights(0, lambda to: gate_hbm.at[to, upper_half], wg_ref.at[upper_half, own_rows])
     for cp in own_weights:
@@ -398,7 +397,7 @@
             mix_ref.at[x],
             mix_ref.at[x],
             mix_send,
-            mix_recv,
+            mix_recv.at[step % 2],
             device_id={"tp": lax.rem(x + step, NX)},
             device_id_type=MESH_ID,
         ).start()
@@ -419,12 +418,28 @@
 
     loads[9].wait()
     loads[10].wait()
-    arrival(mix_ref.at[pl.ds(0, NX - 1)], mix_recv)
-    mixed_ref[...] = jnp.transpose(mix_ref[...].astype(F32).reshape(NX * HW, TOK)).astype(BF16)
+
+    def turned(k):
+        return jnp.transpose(mix_ref[lax.rem(x + k, NX)].astype(F32)).astype(BF16)
+
+    mixed_ref[0] = turned(0)
+    arrival(mix_ref.at[pl.ds(0, 2)], mix_recv.at[1])
+    mixed_ref[1] = turned(1)
+    mixed_ref[2] = turned(3)
+
+    @pl.loop(0, NX)
+    def _(n):
+        columns = quarter_of(n)
+        part = res_ref[:, columns].astype(F32)
+        for m, k in enumerate((0, 1, 3)):
+            part = part + nn(mixed_ref[m], wo_ref[lax.rem(x + k, NX), :, columns])
+        stream_ref[n] = part
+
+    arrival(mix_ref.at[0], mix_recv.at[0])
+    mixed_ref[3] = turned(2)
 
     def project(n, total):
-        columns = quarter_of(n)
-        part = res_ref[:, columns].astype(F32) + nn(mixed_ref[...], wo_ref[:, columns])
+        part = stream_ref[n] + nn(mixed_ref[3], wo_ref[lax.rem(x + 2, NX), :, quarter_of(n)])
         stream_ref[n] = part
         return total + jnp.sum(part * part, axis=1, keepdims=True)
 
@@ -465,17 +480,21 @@
                     sbuf_ref.at[i * PLANE + to], rbuf_ref.at[i * PLANE + p], d_recv.at[i]
                 ).start()
 
-    arrival(sd_ref.at[pl.ds(0, (NX - 1) * (GROUP // NC))], wrecv_sem.at[3])
+    arrival(sd_ref.at[pl.ds(0, (NX - 1) * PART)], wrecv_sem.at[3])
     for step in range(1, NX):
-        rows = core_rows(lax.rem(x + step, NX))
-        pltpu.make_async_remote_copy(
-            sd_ref.at[rows],
-            sd_ref.at[rows],
-            swap_send,
-            swap_recv,
-            device_id={"sp_2": 1 - c},
-            device_id_type=MESH_ID,
-        ).start()
+        rows = part_rows(lax.rem(x + step, NX))
+
+        @pl.loop(1, PLANE)
+        def _(n):
+            pltpu.make_async_remote_copy(
+                sd_ref.at[rows],
+                sd_ref.at[rows],
+                swap_send,
+                swap_recv,
+                device_id=sp_dev(z, lax.rem(p + n, PLANE)),
+                device_id_type=MESH_ID,
+            ).start()
+
     for n in range(11, 14):
         loads[n].wait()
     normed = normed_ref[...]
@@ -545,15 +564,6 @@
             for m in range(result.shape[0]):
                 eo_ref[s, n, :, k + m] = result[m]
 
-    def both_back(s, columns):
-        out_of_expert(s, 0, hidden_ref[s], columns)
-        send_back(
-            lambda to_x, to: eo_ref.at[s, to_x, to],
-            near_ref.at[s, p * NX + x],
-            b_recv.at[2 * s],
-            columns,
-        )
-
     def one_back(i, columns):
         s, k = i // 2, i % 2
         rows = hidden_ref[s, k * (PLANE * CAP) : (k + 1) * (PLANE * CAP)]
@@ -592,23 +602,30 @@
         ).start()
 
     soon, every = (1, 3, 0), (2, 1, 3, 0)
+
+    def returned(i):
+        arrival(near_ref.at[i // 2, :, i % 2], b_recv.at[i])
+
     one_back(0, soon)
-    one_back(1, soon)
     arrival(wd_ref.at[pl.ds(0, FF - GROUP), pl.ds(0, QUARTER)], wrecv_sem.at[4])
     one_back(0, (2,))
-    one_back(1, (2,))
-    both_back(1, every)
-    both_back(2, every)
-    arrival(near_ref.at[0, :, 0], b_recv.at[0])
+    one_back(1, every)
+    one_back(2, every)
+    one_back(3, every)
+    returned(0)
     passed_on(0, 0, None, True)
     passed_on(0, 1, None, False)
-    arrival(near_ref.at[0, :, 1], b_recv.at[1])
+    one_back(4, every)
+    returned(1)
     passed_on(1, 0, None, False)
-    one_back(6, every)
-    arrival(near_ref.at[1], b_recv.at[2])
+    one_back(5, every)
+    returned(2)
     passed_on(2, 1, None, True)
     passed_on(2, 0, 0, True)
     passed_on(1, 1, 0, False)
+    one_back(6, every)
+    returned(3)
+    passed_on(3, 0, 1, False)
     one_back(7, every)
     for step in (2, 1, 3):
         pltpu.make_async_remote_copy(
@@ -619,13 +636,13 @@
             device_id={"tp": lax.rem(x + step, NX)},
             device_id_type=MESH_ID,
         ).start()
-    passed_on(3, 0, 1, False)
-    arrival(near_ref.at[2], b_recv.at[4])
+    returned(4)
     passed_on(4, 1, 2, True)
     passed_on(3, 1, 1, False)
     passed_on(4, 0, 2, True)
+    returned(5)
     passed_on(5, 0, 3, False)
-    arrival(near_ref.at[3, :, 0], b_recv.at[6])
+    returned(6)
     passed_on(6, 1, 4, True)
     passed_on(5, 1, 3, False)
     passed_on(6, 0, 4, True)
@@ -634,7 +651,7 @@
     totals = []
     for h in range(2):
         totals.append(stream_ref[x, :, h * width : (h + 1) * width] + weighted(NZ - 1, h))
-    arrival(sd_ref.at[pl.ds(0, (NX - 1) * (GROUP // NC))], swap_recv)
+    arrival(sd_ref.at[pl.ds(0, (NX - 1) * (GROUP - PART))], swap_recv)
     arrival(shared_ref.at[:, pl.ds(0, FF - GROUP)], rs_rsem)
     for h in range(2):
         columns = slice(h * width, (h + 1) * width)
@@ -653,8 +670,8 @@
     arrival(table_ref.at[pl.ds(0, NZ - 1)], st_send.at[3])
     for n in range(NZ // 2):
         arrival(near_ref.at[n, pl.ds(0, NX * PLANE - 1)], b_send)
-    arrival(sd_ref.at[pl.ds(0, (NX - 1) * (GROUP // NC))], wsend_sem.at[3])
-    arrival(sd_ref.at[pl.ds(0, (NX - 1) * (GROUP // NC))], swap_send)
+    arrival(sd_ref.at[pl.ds(0, (NX - 1) * PART)], wsend_sem.at[3])
+    arrival(sd_ref.at[pl.ds(0, (NX - 1) * (GROUP - PART))], swap_send)
     arrival(shared_ref.at[:, pl.ds(0, FF - GROUP)], rs_ssem)
     arrival(chain_out_ref, chain_send)
 
@@ -702,7 +719,7 @@
             pltpu.VMEM((2, TOK), F32),
             pltpu.VMEM((2, TOK), F32),
             pltpu.VMEM((2, TOK), F32),
-            pltpu.VMEM((NX * HW, D), BF16),
+            pltpu.VMEM((NX, HW, D), BF16),
             pltpu.VMEM((TOK, D), BF16),
             pltpu.VMEM((4, TOK), jnp.int32),
             pltpu.VMEM((4, TOK), F32),
@@ -718,7 +735,7 @@
             pltpu.VMEM((PLANE, SLICE, LANES), F32),
             pltpu.VMEM((PLANE, SLICE, LANES), F32),
             pltpu.VMEM((NX, HW, TOK), BF16),
-            pltpu.VMEM((TOK, NX * HW), BF16),
+            pltpu.VMEM((NX, TOK, HW), BF16),
             pltpu.VMEM((NZ // 2, CHUNK * CAP, FF), BF16),
             pltpu.VMEM((NX, TOK, QUARTER), F32),
             pltpu.VMEM((TOK, D), BF16),
@@ -740,7 +757,7 @@
             dma((4,)),
             dma((4,)),
             dma,
-            dma,
+            dma((2,)),
             dma,
             dma((NZ,)),
             dma,
@@ -766,7 +783,7 @@
         head_forget_bias,
         forget_extra_boost,
         head_norm_gain.reshape(1, HW),
-        memory_output_weight,
+        memory_output_weight.reshape(NX, HW, D),
         residual,
         expert_norm_gain.reshape(1, D),
         routes.T,

time: 125 us -> 120 us (0.960)
  Pallas kernels: 123 us -> 119 us
    pallas_call x1, Pallas kernels: 123 us -> 119 us  [body(): pl.pallas_call(kernel, out_shape=jax.ShapeDtypeStruct((TOK, QUARTER), BF1...]
where the time goes in v3:
time: 120 us
  Pallas kernels  119 us (99%)
  local copies, waits for them, and re-layouts  1.67 us (1%)
    pallas_call x1, Pallas kernels, body(): pl.pallas_call(kernel, out_shape=jax.ShapeDtypeStruct((TOK, QUARTER), BF1...  119 us

profile of v3, /device:TPU:1, one launch (start us, length us, event | category | flops | bytes accessed | tf_op | source)
XLA Modules:
  0.0 120.3 jit_solution(16042969483739209084)
XLA Ops:
  0.0 118.6 %layer.1 = bf16[256,512]{1,0:T(8,128)(2,1)} custom-call(bf16[192,256]{1,0:T(8,128)(2,1)} %bitcast.10, bf16[192,256]{1,0:T(8,128)(2,1)} %bitcast.11, bf16[192,256]{1,0:T(8,128)(2,1)} %bitcast.12, bf16[192,256]{1,0:T(8,128)(2,1)} %bitcast.13, f32[2,256]{1,0:T(2,128)} %lig_hbm.1, f32[2,256]{1,0:T(2,128)} %fpre_hbm.1, f32[2]{0:T(128)} %bias_ref.1, ...), custom_call_target="tpu_custom_call" | custom-call | tf_op jit(solution)/shard_map/layer/pallas_call | solution.py:709
  118.6 1.7 %copy.22 = bf16[256,512]{1,0:T(8,128)(2,1)} copy(bf16[256,512]{1,0:T(8,128)(2,1)} %layer.1) | data formatting | bytes 524288

commit v4 on v3

--- a/solution.py
+++ b/solution.py
@@ -526,8 +526,7 @@
     arrival(wg_ref.at[:, pl.ds(0, FF - GROUP)], wrecv_sem.at[0])
     arrival(wu_ref.at[:, pl.ds(0, FF - GROUP)], wrecv_sem.at[1])
 
-    @pl.loop(0, NZ // 2)
-    def _(s):
+    def hidden_of(s):
         arrival(rbuf_ref.at[pl.ds(0, PLANE)], d_recv.at[2 * s])
         arrival(rbuf_ref.at[pl.ds(0, PLANE)], d_recv.at[2 * s + 1])
         blocks = pl.ds(pl.multiple_of(s * CHUNK, CHUNK), CHUNK)
@@ -535,7 +534,7 @@
         hidden = jax.nn.silu(nn(rows, wg_ref[...])) * nn(rows, wu_ref[...])
         hidden_ref[s] = hidden.astype(BF16)
 
-    arrival(wd_ref.at[pl.ds(0, FF - GROUP), pl.ds(0, D - QUARTER)], wrecv_sem.at[2])
+    pl.loop(0, NZ // 2 - 1)(hidden_of)
 
     def send_back(src, dst, sem, columns):
         for j in columns:
@@ -606,7 +605,9 @@
     def returned(i):
         arrival(near_ref.at[i // 2, :, i % 2], b_recv.at[i])
 
+    arrival(wd_ref.at[pl.ds(0, FF - GROUP), pl.ds(0, D - QUARTER)], wrecv_sem.at[2])
     one_back(0, soon)
+    hidden_of(NZ // 2 - 1)
     arrival(wd_ref.at[pl.ds(0, FF - GROUP), pl.ds(0, QUARTER)], wrecv_sem.at[4])
     one_back(0, (2,))
     one_back(1, every)
@@ -653,7 +654,7 @@
         totals.append(stream_ref[x, :, h * width : (h + 1) * width] + weighted(NZ - 1, h))
     arrival(sd_ref.at[pl.ds(0, (NX - 1) * (GROUP - PART))], swap_recv)
     arrival(shared_ref.at[:, pl.ds(0, FF - GROUP)], rs_rsem)
-    for h in range(2):
+    for h in (1, 0):
         columns = slice(h * width, (h + 1) * width)
         total = totals[h] + nn(shared_ref[...], sd_ref[:, columns])
         total = total + arrived(5, h) + arrived(6, h)

time: 120 us -> 119 us (level)
  no operation moved by 1% of the time
where the time goes in v4:
time: 119 us
  Pallas kernels  118 us (99%)
  local copies, waits for them, and re-layouts  1.67 us (1%)
    pallas_call x1, Pallas kernels, body(): pl.pallas_call(kernel, out_shape=jax.ShapeDtypeStruct((TOK, QUARTER), BF1...  118 us

profile of v4, /device:TPU:1, one launch (start us, length us, event | category | flops | bytes accessed | tf_op | source)
XLA Modules:
  0.0 119.2 jit_solution(5329554162026489285)
XLA Ops:
  0.0 117.5 %layer.1 = bf16[256,512]{1,0:T(8,128)(2,1)} custom-call(bf16[192,256]{1,0:T(8,128)(2,1)} %bitcast.10, bf16[192,256]{1,0:T(8,128)(2,1)} %bitcast.11, bf16[192,256]{1,0:T(8,128)(2,1)} %bitcast.12, bf16[192,256]{1,0:T(8,128)(2,1)} %bitcast.13, f32[2,256]{1,0:T(2,128)} %lig_hbm.1, f32[2,256]{1,0:T(2,128)} %fpre_hbm.1, f32[2]{0:T(128)} %bias_ref.1, ...), custom_call_target="tpu_custom_call" | custom-call | tf_op jit(solution)/shard_map/layer/pallas_call | solution.py:710
  117.5 1.7 %copy.22 = bf16[256,512]{1,0:T(8,128)(2,1)} copy(bf16[256,512]{1,0:T(8,128)(2,1)} %layer.1) | data formatting | bytes 524288

commit v5 on v4

--- a/solution.py
+++ b/solution.py
@@ -423,23 +423,21 @@
         return jnp.transpose(mix_ref[lax.rem(x + k, NX)].astype(F32)).astype(BF16)
 
     mixed_ref[0] = turned(0)
-    arrival(mix_ref.at[pl.ds(0, 2)], mix_recv.at[1])
-    mixed_ref[1] = turned(1)
-    mixed_ref[2] = turned(3)
 
     @pl.loop(0, NX)
     def _(n):
         columns = quarter_of(n)
-        part = res_ref[:, columns].astype(F32)
-        for m, k in enumerate((0, 1, 3)):
-            part = part + nn(mixed_ref[m], wo_ref[lax.rem(x + k, NX), :, columns])
-        stream_ref[n] = part
-
+        stream_ref[n] = res_ref[:, columns].astype(F32) + nn(mixed_ref[0], wo_ref[x, :, columns])
+
+    arrival(mix_ref.at[pl.ds(0, 2)], mix_recv.at[1])
     arrival(mix_ref.at[0], mix_recv.at[0])
-    mixed_ref[3] = turned(2)
+    for k in range(1, NX):
+        mixed_ref[k] = turned(k)
 
     def project(n, total):
-        part = stream_ref[n] + nn(mixed_ref[3], wo_ref[lax.rem(x + 2, NX), :, quarter_of(n)])
+        part = stream_ref[n]
+        for k in range(1, NX):
+            part = part + nn(mixed_ref[k], wo_ref[lax.rem(x + k, NX), :, quarter_of(n)])
         stream_ref[n] = part
         return total + jnp.sum(part * part, axis=1, keepdims=True)
 

time: 119 us -> 120 us (level)
  no operation moved by 1% of the time
where the time goes in v5:
time: 120 us; the launch traced here: 119 us
  Pallas kernels  118 us (98%)
  local copies, waits for them, and re-layouts  1.67 us (1%)
    pallas_call x1, Pallas kernels, body(): pl.pallas_call(kernel, out_shape=jax.ShapeDtypeStruct((TOK, QUARTER), BF1...  118 us

profile of v5, /device:TPU:1, one launch (start us, length us, event | category | flops | bytes accessed | tf_op | source)
XLA Modules:
  0.0 119.5 jit_solution(10288160041892400270)
XLA Ops:
  0.0 117.8 %layer.1 = bf16[256,512]{1,0:T(8,128)(2,1)} custom-call(bf16[192,256]{1,0:T(8,128)(2,1)} %bitcast.10, bf16[192,256]{1,0:T(8,128)(2,1)} %bitcast.11, bf16[192,256]{1,0:T(8,128)(2,1)} %bitcast.12, bf16[192,256]{1,0:T(8,128)(2,1)} %bitcast.13, f32[2,256]{1,0:T(2,128)} %lig_hbm.1, f32[2,256]{1,0:T(2,128)} %fpre_hbm.1, f32[2]{0:T(128)} %bias_ref.1, ...), custom_call_target="tpu_custom_call" | custom-call | tf_op jit(solution)/shard_map/layer/pallas_call | solution.py:708
  117.8 1.7 %copy.22 = bf16[256,512]{1,0:T(8,128)(2,1)} copy(bf16[256,512]{1,0:T(8,128)(2,1)} %layer.1) | data formatting | bytes 524288
